TPU v7x, 256 devices: a whole 4x4x8 slice. The times are simulated.
256 devices in a mesh: sp: 16 (over y, x), tp: 16 (over z, core).
Axes of the slice: x: 4, y: 4, z: 8, core: 2. Of those that a mesh axis runs over, the one named last changes fastest.
Arguments:
- layer_input: bfloat16 [8192, 2048], P(('sp', 'tp')), may hold values from -6 to 6
- receptance: bfloat16 [8192, 2048], P('sp', 'tp'), may hold values from -6 to 6
- keys: bfloat16 [8192, 2048], P('sp', 'tp'), may hold values from -6 to 6
- values: bfloat16 [8192, 2048], P('sp', 'tp'), may hold values from -6 to 6
- erase_preact: bfloat16 [8192, 2048], P('sp', 'tp'), may hold values from -12 to 5
- decay_preact: bfloat16 [8192, 2048], P('sp', 'tp'), may hold values from -40 to 3
- decay_spike: float32 [8192, 32], P('sp', 'tp'), may hold values from -2 to 0
- head_norm_gain: bfloat16 [2048], P('tp'), may hold values from 0.099609375 to 1.8984375
- output_weight: bfloat16 [2048, 2048], P('tp'), may hold values from -0.125 to 0.125
- expert_norm_gain: bfloat16 [2048], replicated, may hold values from 0.099609375 to 1.8984375
- routes: int32 [8192, 2], P(('sp', 'tp')), may hold values from 0 to 31, all different within a row; in each aligned block of 32 rows (0 to 31, 32 to 63, ...) at most 3 rows name the same one
- routing_weight: float32 [8192, 2], P(('sp', 'tp')), may hold values from 0.3 to 1.5
- expert_gate_weight: bfloat16 [32, 2048, 4096], P('sp', None, 'tp'), may hold values from -0.125 to 0.125
- expert_up_weight: bfloat16 [32, 2048, 4096], P('sp', None, 'tp'), may hold values from -0.125 to 0.125
- expert_down_weight: bfloat16 [32, 4096, 2048], P('sp', 'tp'), may hold values from -0.09375 to 0.09375
- shared_gate_weight: bfloat16 [2048, 4096], P(None, 'tp'), may hold values from -0.125 to 0.125
- shared_up_weight: bfloat16 [2048, 4096], P(None, 'tp'), may hold values from -0.125 to 0.125
- shared_down_weight: bfloat16 [4096, 2048], P('tp'), may hold values from -0.09375 to 0.09375
Outputs:
- layer_out: bfloat16 [8192, 2048], P(('sp', 'tp'))
Inputs may be any that keep to these rules, and one draw needn't show every extreme that they name: `routes`: in each aligned block of 32 rows no expert is named by more than 3 rows.
All inputs are finite; a program needn't handle non-finite values.
Results may differ from a plain program's by a relative error of at most 0.02.
Values may be sent and summed in bfloat16 or wider, within the bound.
A program may use at most 128 MiB of HBM per device.

v0:
```python
import jax
import jax.numpy as jnp
from jax import lax
from jax.sharding import Mesh
from jax.sharding import PartitionSpec as P

BLOCK = 64
SP = ("sp_0", "sp_1")
TP = ("tp_0", "tp_1")
SP_TP = ("sp_0", "sp_1", "tp_0", "tp_1")


highest = lax.Precision.HIGHEST
GN_EPS = 0.00064
RMS_EPS = 1e-06


def nothing_yet(array, identity):
    return jax.tree.map(
        lambda a, e: jnp.broadcast_to(jnp.asarray(e, a.dtype), a.shape), array, identity
    )


def gathered_once(array, axis):
    leaves = jax.tree.leaves(array)
    turns = sorted(range(len(leaves)), key=lambda k: -leaves[k].size)
    width = (1, *leaves[turns[0]].shape)[-1]
    lines = [
        jnp.pad(leaves[k].reshape(-1), (0, -leaves[k].size % width)).reshape(-1, width)
        for k in turns
    ]
    both, at, found = (lax.all_gather(jnp.concatenate(lines), axis), 0, {})
    for k, line in zip(turns, lines):
        section = both[:, at : at + len(line)].reshape(len(both), -1)
        found[k] = section[:, : leaves[k].size].reshape(-1, *leaves[k].shape)
        at += len(line)
    numbers = iter(range(len(leaves)))
    return jax.tree.map(lambda _: found[next(numbers)], array)


def prefix_by_axis(array, axes, combine, identity, reverse):
    before = start = nothing_yet(array, identity)
    so_far = array
    for axis in reversed(axes):
        size, place = (lax.axis_size(axis), lax.axis_index(axis))
        pieces = gathered_once(
            jax.tree.map(
                lambda part, kind: part.astype(kind), so_far, (jnp.bfloat16, jnp.bfloat16)
            ),
            axis,
        )
        inside, so_far = (start, start)
        for k in reversed(range(size)) if reverse else range(size):
            passed = k > place if reverse else k < place
            so_far = combine(
                so_far, jax.tree.map(lambda part, own: part[k].astype(own.dtype), pieces, array)
            )
            inside = jax.tree.map(lambda new, old: jnp.where(passed, new, old), so_far, inside)
        before = combine(inside, before)
    return before


def cut_along(array, dim, size):
    before, after = (array.shape[:dim], array.shape[dim + 1 :])
    return jnp.moveaxis(array.reshape(*before, size, -1, *after), dim, 0)


def laid_out(tiles, dim):
    tiles = jnp.moveaxis(tiles, 0, dim)
    dims = tiles.shape
    return tiles.reshape(*dims[:dim], dims[dim] * dims[dim + 1], *dims[dim + 2 :])


def turned_blocks(tiles, axes, turns):
    inside = tiles.shape[1:]
    whole = tiles.reshape(*(lax.axis_size(a) for a in axes), *inside)
    for k in turns:
        whole = lax.all_to_all(whole, axes[k], k, k, tiled=True)
    return whole.reshape(-1, *inside)


def exchange_by_axis(array, axes, turns, split_dim, concat_dim):
    tiles = cut_along(array, split_dim, lax.axis_size(axes))
    return laid_out(turned_blocks(tiles, axes, turns), concat_dim)


def chain_product(left_mat, right_mat):
    return jnp.einsum("...ij,...jk->...ik", left_mat, right_mat, precision=highest)


def compose(earlier, later):
    return (chain_product(earlier[0], later[0]), chain_product(earlier[1], later[0]) + later[1])


def block_terms(decay_logarithm, unit_keys, beta, key_rows, value_rows, read_rows, span_len):
    tokens_here, head_number, head_width = key_rows.shape
    block_count = tokens_here // span_len

    def to_blocks(array):
        return jnp.swapaxes(array.reshape(block_count, span_len, head_number, head_width), 1, 2)

    decay_logarithm, unit_keys, beta, key_rows, value_rows, read_rows = [
        to_blocks(array)
        for array in (decay_logarithm, unit_keys, beta, key_rows, value_rows, read_rows)
    ]
    cumulative = jnp.cumsum(decay_logarithm, axis=2)
    ending = cumulative[:, :, -1:, :]
    unit_scaled = unit_keys * jnp.exp(cumulative - decay_logarithm)
    read_scaled = read_rows * jnp.exp(cumulative)
    beta_scaled = beta * jnp.exp(-cumulative)
    key_scaled = key_rows * jnp.exp(-cumulative)
    row_ids = lax.broadcasted_iota(jnp.int32, (span_len, span_len), 0)
    col_ids = lax.broadcasted_iota(jnp.int32, (span_len, span_len), 1)

    def pairs(left_rows, right_rows, keep):
        return jnp.where(
            keep, jnp.einsum("bhtn,bhsn->bhts", left_rows, right_rows, precision=highest), 0.0
        )

    def apply_rows(weights, rows_in):
        return jnp.einsum("bhts,bhsn->bhtn", weights, rows_in, precision=highest)

    erase_beta = pairs(unit_scaled, beta_scaled, row_ids > col_ids)
    erase_key = pairs(unit_scaled, key_scaled, row_ids > col_ids)
    read_beta = pairs(read_scaled, beta_scaled, row_ids >= col_ids)
    read_key = pairs(read_scaled, key_scaled, row_ids >= col_ids)
    triangle = erase_beta + (row_ids == col_ids).astype(jnp.float32)
    right_side = jnp.concatenate([unit_scaled, -apply_rows(erase_key, value_rows)], axis=-1)
    solved = jax.scipy.linalg.solve_triangular(triangle, right_side, lower=True, unit_diagonal=True)
    lead_rows = solved[..., :head_width]
    own_rows = solved[..., head_width:]
    local = apply_rows(read_beta, own_rows) + apply_rows(read_key, value_rows)
    readout = read_scaled - apply_rows(read_beta, lead_rows)
    beta_end = beta * jnp.exp(ending - cumulative)
    key_end = key_rows * jnp.exp(ending - cumulative)
    diagonal = jnp.exp(ending)[:, :, 0, :, None] * jnp.eye(head_width, dtype=jnp.float32)
    transition = diagonal - jnp.einsum("bhtn,bhtm->bhnm", lead_rows, beta_end, precision=highest)
    carried = jnp.einsum("bhtv,bhtm->bhvm", own_rows, beta_end, precision=highest) + jnp.einsum(
        "bhtv,bhtm->bhvm", value_rows, key_end, precision=highest
    )
    return (local, readout, transition, carried)


def block_chain(transition, carried):
    head_number, head_width = (transition.shape[1], transition.shape[2])
    identity = jnp.broadcast_to(
        jnp.eye(head_width, dtype=jnp.float32), (head_number, head_width, head_width)
    )

    def advance(running, block_pair):
        product, state_now = running
        updated = (
            chain_product(product, block_pair[0]),
            chain_product(state_now, block_pair[0]) + block_pair[1],
        )
        return (updated, (product, state_now))

    (whole_map, ending), (prefix, starts) = lax.scan(
        advance, (identity, jnp.zeros_like(identity)), (transition, carried)
    )
    return (whole_map, ending, prefix, starts)


def sweep(arrays, span_len):
    local, readout, transition, carried = block_terms(*arrays, span_len)
    whole_map, ending, prefix, starts = block_chain(transition, carried)
    return ((local, readout, prefix, starts), (whole_map, ending))


def finish(parts, entry):
    local, readout, prefix, starts = parts
    start_state = jnp.einsum("hvn,bhnm->bhvm", entry, prefix, precision=highest) + starts
    result = local + jnp.einsum("bhtn,bhvn->bhtv", readout, start_state, precision=highest)
    return jnp.swapaxes(result, 1, 2).reshape(-1, result.shape[1], result.shape[3])


def body(
    layer_input,
    receptance,
    keys,
    values,
    erase_preact,
    decay_preact,
    decay_spike,
    head_norm_gain,
    output_weight,
    expert_norm_gain,
    routes,
    routing_weight,
    expert_gate_weight,
    expert_up_weight,
    expert_down_weight,
    shared_gate_weight,
    shared_up_weight,
    shared_down_weight,
):
    tokens_here = keys.shape[0]
    head_number = decay_spike.shape[1]
    head_width = keys.shape[1] // head_number

    def each_head(array):
        return array.astype(jnp.float32).reshape(tokens_here, head_number, head_width)

    key_rows = each_head(keys)
    unit_keys = key_rows * lax.rsqrt(jnp.sum(key_rows * key_rows, axis=-1, keepdims=True) + 1e-06)
    beta = unit_keys * jax.nn.sigmoid(each_head(erase_preact))
    decay_logarithm = (
        -jnp.exp(-jax.nn.softplus(-each_head(decay_preact)) - 0.5) + decay_spike[:, :, None]
    )
    arrays = (decay_logarithm, unit_keys, beta, key_rows, each_head(values), each_head(receptance))
    forward_parts, forward_map = sweep(arrays, BLOCK)
    backward_parts, backward_map = sweep(tuple((array[::-1] for array in arrays)), BLOCK)
    identity = jnp.broadcast_to(jnp.eye(head_width, dtype=jnp.float32), forward_map[0].shape)
    blank = jnp.zeros_like(forward_map[1])
    forward_entry = prefix_by_axis(
        (forward_map[0], forward_map[1]), SP, compose, (identity, blank), False
    )[1]
    backward_entry = prefix_by_axis(
        (backward_map[0], backward_map[1]), SP, compose, (identity, blank), True
    )[1]
    mix = finish(forward_parts, forward_entry) + finish(backward_parts, backward_entry)[::-1]
    center = jnp.mean(mix, axis=-1, keepdims=True)
    spread = jnp.mean(jnp.square(mix - center), axis=-1, keepdims=True)
    mixed = ((mix - center) * lax.rsqrt(spread + GN_EPS)).reshape(
        tokens_here, head_number * head_width
    )
    mixed = (mixed * head_norm_gain.astype(jnp.float32)).astype(jnp.bfloat16)
    row_count = layer_input.shape[0]
    model_width = layer_input.shape[1]
    token_major = exchange_by_axis(mixed, TP, (1, 0), 0, 1)
    projected = jnp.dot(
        token_major,
        lax.all_gather(output_weight, TP, axis=0, tiled=True),
        preferred_element_type=jnp.float32,
    )
    residual = layer_input.astype(jnp.float32) + projected
    normed = residual * lax.rsqrt(jnp.mean(residual * residual, axis=-1, keepdims=True) + RMS_EPS)
    normed = (normed * expert_norm_gain.astype(jnp.float32)).astype(jnp.bfloat16)
    top_count = routes.shape[1]
    expert_local = expert_gate_weight.shape[0]
    sp_count = lax.axis_size(SP)
    expert_total = expert_local * sp_count
    capacity = max(2, (3 * row_count * top_count + 2 * expert_total - 1) // (2 * expert_total))
    slot_total = sp_count * capacity * expert_local
    entries = routes.reshape(-1)
    entry_count = entries.shape[0]
    expert_hot = (entries[:, None] == lax.broadcasted_iota(jnp.int32, (1, expert_total), 1)).astype(
        jnp.int32
    )
    rank_in = jnp.sum((jnp.cumsum(expert_hot, axis=0) - 1) * expert_hot, axis=1)
    slot_of = (entries // expert_local * capacity + rank_in) * expert_local + entries % expert_local
    slot_hot = (slot_of[:, None] == lax.broadcasted_iota(jnp.int32, (1, slot_total), 1)).astype(
        jnp.float32
    )
    owner_hot = (
        lax.broadcasted_iota(jnp.int32, (entry_count, 1), 0) // top_count
        == lax.broadcasted_iota(jnp.int32, (1, row_count), 1)
    ).astype(jnp.float32)
    placing = jnp.dot(slot_hot.T, owner_hot, precision=highest)
    weighting = jnp.dot(owner_hot.T, slot_hot * routing_weight.reshape(-1, 1), precision=highest)
    outgoing = jnp.dot(placing.astype(jnp.bfloat16), normed, preferred_element_type=jnp.float32)
    outgoing = outgoing.astype(jnp.bfloat16).reshape(sp_count, capacity, expert_local, model_width)
    arrived = lax.all_to_all(outgoing, SP, split_axis=0, concat_axis=0, tiled=True)
    own_block = jnp.concatenate([arrived.reshape(slot_total, model_width), normed], axis=0)
    block_rows = own_block.shape[0]
    everyone = lax.all_gather(own_block, TP, axis=0, tiled=True)
    slab = everyone
    slab = slab.reshape(block_rows * lax.axis_size(TP) // block_rows, block_rows, model_width)
    routed_in = slab[:, :slot_total].reshape(-1, expert_local, model_width)
    gate_value = jnp.einsum(
        "rjd,jdh->rjh", routed_in, expert_gate_weight, preferred_element_type=jnp.float32
    )
    up_value = jnp.einsum(
        "rjd,jdh->rjh", routed_in, expert_up_weight, preferred_element_type=jnp.float32
    )
    hidden = (jax.nn.silu(gate_value) * up_value).astype(jnp.bfloat16)
    routed_out = jnp.einsum(
        "rjh,jhd->rjd", hidden, expert_down_weight, preferred_element_type=jnp.float32
    )
    routed_out = routed_out.reshape(-1, slot_total, model_width)
    shared_in = slab[:, slot_total:].reshape(-1, model_width)
    shared_hidden = (
        jax.nn.silu(jnp.dot(shared_in, shared_gate_weight, preferred_element_type=jnp.float32))
        * jnp.dot(shared_in, shared_up_weight, preferred_element_type=jnp.float32)
    ).astype(jnp.bfloat16)
    shared_out = jnp.dot(shared_hidden, shared_down_weight, preferred_element_type=jnp.float32)
    shared_out = shared_out.reshape(-1, row_count, model_width)
    summed = lax.psum_scatter(
        jnp.concatenate([routed_out, shared_out], axis=1)
        .reshape(block_rows * lax.axis_size(TP), model_width)
        .astype(jnp.bfloat16),
        TP,
        scatter_dimension=0,
        tiled=True,
    ).astype(jnp.float32)
    routed_rows = (
        summed[:slot_total]
        .astype(jnp.bfloat16)
        .reshape(sp_count, capacity, expert_local, model_width)
    )
    returned = lax.all_to_all(routed_rows, SP, split_axis=0, concat_axis=0, tiled=True)
    routed = jnp.dot(
        weighting, returned.reshape(slot_total, model_width).astype(jnp.float32), precision=highest
    )
    return (residual + summed[slot_total:] + routed).astype(jnp.bfloat16)


def solution(mesh):
    finer = Mesh(mesh.devices.reshape(4, 4, 8, 2), ("sp_0", "sp_1", "tp_0", "tp_1"))
    in_specs = (
        P(SP_TP, None),
        P(SP, TP),
        P(SP, TP),
        P(SP, TP),
        P(SP, TP),
        P(SP, TP),
        P(SP, TP),
        P(TP),
        P(TP, None),
        P(),
        P(SP_TP, None),
        P(SP_TP, None),
        P(SP, None, TP),
        P(SP, None, TP),
        P(SP, TP, None),
        P(None, TP),
        P(None, TP),
        P(TP, None),
    )
    out_specs = P(SP_TP, None)
    return jax.shard_map(body, mesh=finer, in_specs=in_specs, out_specs=out_specs, check_vma=False)
```

profile of v0, /device:TPU:6, one launch (start us, length us, event | category | flops | bytes accessed | tf_op | source)
XLA Modules:
  0.0 638.6 jit_solution(12790525818129190324)
XLA Ops:
  33.2 2.4 convolution_bitcast_fusion.6
  43.3 80.5 %custom-call.6 = f32[8,2,1,64,64]{3,4,2,1,0:T(8,128)} custom-call(f32[8,2,1,64,64]{4,3,2,1,0:T(8,128)} %fusion.46), custom_call_target="InvertDiagBlocksLowerTriangular" | custom-call | tf_op jit(solution)/shard_map/jit(_solve_triangular)/vmap(vmap())/triangular_solve | solution.py:129
  123.8 2.6 fusion.59
  134.3 18.0 %while.34 = (s32[]{:T(128)}, f32[2,64,64]{1,2,0:T(8,128)S(1)}, f32[2,64,64]{1,2,0:T(8,128)S(1)}, f32[8,2,64,64]{2,3,1,0:T(8,128)}, f32[8,2,64,64]{2,3,1,0:T(8,12...) while((s32[]{:T(128)}, f32[2,64,64]{1,2,0:T(8,128)S(1)}, ...), condition=%wide.region_3.5_spmd.clone, body=%wide.region_2.4_spmd.clone.sunk | while | flops 12607491 | bytes 852096 | solution.py:158
  152.7 12.0 %all-gather = bf16[1024,64]{0,1:T(8,128)(2,1)S(1)} all-gather(bf16[256,64]{0,1:T(8,128)(2,1)S(1)} %pad_maximum_fusion.4), channel_id=2, replica_groups=mesh['sp_0'=4,'sp_1'=4,'tp_0'=8,'tp_1'=2] {'sp_1'}, dimensions={0}, use_global_device_ids=true | all-gather | bytes 163840 | tf_op jit(solution)/shard_map/all_gather | solution.py:32
  166.3 12.8 %all-gather.1 = bf16[1024,64]{1,0:T(8,128)(2,1)S(1)} all-gather(bf16[256,64]{1,0:T(8,128)(2,1)S(1)} %pad_maximum_fusion.2), channel_id=3, replica_groups=mesh['sp_0'=4,'sp_1'=4,'tp_0'=8,'tp_1'=2] {'sp_0'}, dimensions={0}, use_global_device_ids=true | all-gather | bytes 163840 | tf_op jit(solution)/shard_map/all_gather | solution.py:32
  196.6 3.1 rev.21
  201.9 3.1 rev.24
  216.2 79.3 %custom-call.7 = f32[8,2,1,64,64]{3,4,2,1,0:T(8,128)} custom-call(f32[8,2,1,64,64]{4,3,2,1,0:T(8,128)S(1)} %fusion.44), custom_call_target="InvertDiagBlocksLowerTriangular" | custom-call | tf_op jit(solution)/shard_map/jit(_solve_triangular)/vmap(vmap())/triangular_solve | solution.py:129
  295.5 2.6 fusion.63
  306.0 31.7 %while.35 = (s32[]{:T(128)}, f32[2,64,64]{1,2,0:T(8,128)S(1)}, f32[2,64,64]{1,2,0:T(8,128)S(1)}, f32[8,2,64,64]{2,3,1,0:T(8,128)}, f32[8,2,64,64]{2,3,1,0:T(8,12...) while((s32[]{:T(128)}, f32[2,64,64]{1,2,0:T(8,128)S(1)}, ...), condition=%wide.region_6.8_spmd.clone, body=%wide.region_5.7_spmd.clone.sunk | while | flops 12607491 | bytes 753792 | solution.py:158
  338.0 12.0 %all-gather.2 = bf16[1024,64]{0,1:T(8,128)(2,1)S(1)} all-gather(bf16[256,64]{0,1:T(8,128)(2,1)S(1)} %pad_maximum_fusion.5), channel_id=4, replica_groups=mesh['sp_0'=4,'sp_1'=4,'tp_0'=8,'tp_1'=2] {'sp_1'}, dimensions={0}, use_global_device_ids=true | all-gather | bytes 163840 | tf_op jit(solution)/shard_map/all_gather | solution.py:32
  353.1 12.3 %all-gather.3 = bf16[1024,64]{1,0:T(8,128)(2,1)S(1)} all-gather(bf16[256,64]{1,0:T(8,128)(2,1)S(1)} %pad_maximum_fusion.3), channel_id=5, replica_groups=mesh['sp_0'=4,'sp_1'=4,'tp_0'=8,'tp_1'=2] {'sp_0'}, dimensions={0}, use_global_device_ids=true | all-gather | bytes 163840 | tf_op jit(solution)/shard_map/all_gather | solution.py:32
  374.3 3.8 all_to_all.20
  378.8 8.5 %all-to-all-start.1 = ((bf16[8,2,32,128]{3,2,1,0:T(8,128)(2,1)}), bf16[8,2,32,128]{3,2,1,0:T(8,128)(2,1)S(1)}, u32[]{:S(2)}, u32[]{:S(2)}) async-start(bf16[8,2,32,128]{3,2,1,0:T(8,128)(2,1)} %copy.355), calls=%async_computation.1 | async-start | bytes 262144 | tf_op jit(solution)/shard_map/all_to_all | solution.py:78
  388.2 8.5 %all-to-all-done.1 = bf16[8,2,32,128]{3,2,1,0:T(8,128)(2,1)S(1)} async-done(((bf16[8,2,32,128]{3,2,1,0:T(8,128)(2,1)}), bf16[8,2,32,128]{3,2,1,0:T(8,128)(2,1)S(1)}, u32[]{:S(2)}, u32[]{:S(2)}) %all-to-all-start.1) | async-done | bytes 131104 | tf_op jit(solution)/shard_map/all_to_all | solution.py:78
  396.7 5.0 multiply_reduce_fusion
  402.4 13.0 %all_to_all.21 = bf16[16,3,2,2048]{3,2,1,0:T(2,128)(2,1)S(1)} all-to-all(bf16[16,3,2,2048]{3,2,1,0:T(2,128)(2,1)S(1)} %reshape.419), channel_id=1, replica_groups=mesh['sp_0'=4,'sp_1'=4,'tp_0'=8,'tp_1'=2] {'sp_0','sp_1'}, dimensions={0} | all-to-all | bytes 786432 | tf_op jit(solution)/shard_map/all_to_all | solution.py:263
  416.7 50.4 %all-gather.9.cloned.1.call-done = bf16[2048,2048]{1,0:T(8,128)(2,1)} async-done(((bf16[128,2048]{1,0:T(8,128)(2,1)}), bf16[2048,2048]{1,0:T(8,128)(2,1)}) %all-gather.9.cloned.1.call-update) | async-done | bytes 8388624 | tf_op jit(solution)/shard_map/all_gather | solution.py:266
  467.1 3.1 slice.288
  470.2 6.6 %slice.287 = bf16[16,96,2048]{2,1,0:T(8,128)(2,1)} slice(bf16[16,128,2048]{2,1,0:T(8,128)(2,1)} %bitcast.389), slice={[0:16], [0:96], [0:2048]} | slice | bytes 12582912 | tf_op jit(solution)/shard_map/slice | solution.py:269
  476.9 10.9 %reshape.422 = bf16[768,2,2048]{2,1,0:T(2,128)(2,1)} reshape(bf16[16,96,2048]{2,1,0:T(8,128)(2,1)} %slice.287) | data formatting | bytes 12582912 | tf_op jit(solution)/shard_map/reshape | solution.py:269
  487.7 6.5 %fusion.24 = f32[2,768,256]{2,1,0:T(8,128)} fusion(bf16[2,2048,256]{2,1,0:T(8,128)(2,1)} %param.36, bf16[768,2,2048]{2,1,0:T(2,128)(2,1)} %reshape.422), kind=kOutput, calls=%fused_computation.36 | convolution fusion | flops 1610612736 | bytes 9961472 | tf_op jit(solution)/shard_map/rjd,jdh->rjh/dot_general | solution.py:270
  494.2 10.3 %convert_bitcast_fusion = bf16[768,2,2048]{2,0,1:T(8,128)(2,1)} fusion(bf16[2,256,2048]{2,1,0:T(8,128)(2,1)S(1)} %copy-done, f32[2,768,256]{2,1,0:T(8,128)} %fusion.24, bf16[2,2048,256]{2,1,0:T(8,128)(2,1)} %param.37, bf16[768,2,2048]{2,1,0:T(2,128)(2,1)} %reshape.422), kind=kOutput, calls=%fused_computation.33 | convolution fusion | flops 3226730496 | bytes 18350080 | tf_op jit(solution)/shard_map/rjh,jhd->rjd/dot_general | solution.py:277
  504.5 12.6 %copy.360 = bf16[768,2,2048]{2,1,0:T(2,128)(2,1)} copy(bf16[768,2,2048]{2,0,1:T(8,128)(2,1)} %convert_bitcast_fusion) | data formatting | bytes 12582912 | tf_op jit(solution)/shard_map/rjh,jhd->rjd/transpose | solution.py:277
  517.2 10.2 %reshape.423 = bf16[16,96,2048]{2,1,0:T(8,128)(2,1)} reshape(bf16[768,2,2048]{2,1,0:T(2,128)(2,1)} %copy.360) | data formatting | bytes 12582912 | tf_op jit(solution)/shard_map/reshape | solution.py:280
  527.3 2.6 fusion.198
  529.9 5.8 convolution_convert_fusion
  535.7 8.4 %pad_maximum_fusion = bf16[16,128,2048]{2,1,0:T(8,128)(2,1)} fusion(bf16[16,32,2048]{2,1,0:T(8,128)(2,1)} %bitcast.396, bf16[16,96,2048]{2,1,0:T(8,128)(2,1)} %reshape.423), kind=kLoop, calls=%fused_computation.32 | loop fusion | flops 16777216 | bytes 16777216 | tf_op jit(solution)/shard_map/concatenate | solution.py:289
  544.2 69.6 %reduce-scatter.2.cloned.1.call-done = bf16[128,2048]{1,0:T(8,128)(2,1)} async-done(((bf16[2048,2048]{1,0:T(8,128)(2,1)}), bf16[128,2048]{1,0:T(8,128)(2,1)}) %reduce-scatter.2.cloned.1.call-update) | async-done | bytes 524304 | tf_op jit(solution)/shard_map/reduce_scatter | solution.py:288
  615.8 7.1 %all-to-all-start.3 = ((bf16[16,3,2,2048]{3,2,1,0:T(2,128)(2,1)}), bf16[16,3,2,2048]{3,2,1,0:T(2,128)(2,1)S(1)}, u32[]{:S(2)}, u32[]{:S(2)}) async-start(bf16[16,3,2,2048]{3,2,1,0:T(2,128)(2,1)} %reshape.426), calls=%async_computation.4 | async-start | bytes 786432 | tf_op jit(solution)/shard_map/all_to_all | solution.py:301
  623.3 6.3 all-to-all-done.3
  (400 shorter events, 150.9 us)
Async XLA Ops:
  6.5 487.7 %copy-start = (bf16[2,256,2048]{2,1,0:T(8,128)(2,1)S(1)}, bf16[2,256,2048]{2,1,0:T(8,128)(2,1)}, u32[]{:S(2)}) copy-start(bf16[2,256,2048]{2,1,0:T(8,128)(2,1)} %param.38) | copy-start | bytes 6291460
  6.5 4.5 copy-start.34
  6.5 390.1 %all-gather.7.cloned.1.call-start = ((), (), s32[]{:S(2)}) async-start(), calls=%async_computation.5 | async-start | bytes 8912896 | tf_op jit(solution)/shard_map/all_gather | solution.py:233
  11.1 6.5 %copy-start.44 = (f32[512,2]{0,1:T(2,128)S(1)}, f32[512,2]{0,1:T(2,128)}, u32[]{:S(2)}) copy-start(f32[512,2]{0,1:T(2,128)} %param.30) | copy-start | bytes 12292
  28.5 7.0 %copy-start.42 = (f32[512,2]{0,1:T(2,128)}, f32[512,2]{0,1:T(2,128)S(1)}, u32[]{:S(2)}) copy-start(f32[512,2]{0,1:T(2,128)S(1)} %add_rsqrt_fusion.1) | copy-start | bytes 12292
  30.9 4.7 copy-start.15
  30.9 4.6 copy-start.24
  37.1 4.4 copy-start.7
  39.2 4.1 copy-start.40
  41.6 84.9 %copy-start.5 = (f32[8,64,2,64]{3,1,2,0:T(8,128)S(1)}, f32[8,64,2,64]{3,1,2,0:T(8,128)}, u32[]{:S(2)}) copy-start(f32[8,64,2,64]{3,1,2,0:T(8,128)} %copy.267) | copy-start | bytes 786436
  123.8 4.2 copy-start.31
  165.1 15.3 %copy-start.27 = (f32[8,2,64,64]{2,3,1,0:T(8,128)S(1)}, f32[8,2,64,64]{2,3,1,0:T(8,128)}, u32[]{:S(2)}) copy-start(f32[8,2,64,64]{2,3,1,0:T(8,128)} %get-tuple-element.86) | copy-start | bytes 786436
  165.1 15.3 %copy-start.28 = (f32[8,2,64,64]{2,3,1,0:T(8,128)S(1)}, f32[8,2,64,64]{2,3,1,0:T(8,128)}, u32[]{:S(2)}) copy-start(f32[8,2,64,64]{2,3,1,0:T(8,128)} %get-tuple-element.89) | copy-start | bytes 786436
  182.5 5.5 copy-start.21
  182.5 5.5 copy-start.45
  188.6 3.4 copy-start.19
  188.6 3.4 copy-start.43
  199.7 7.4 %copy-start.35 = (bf16[512,128]{0,1:T(8,128)(2,1)S(1)}, bf16[512,128]{0,1:T(8,128)(2,1)}, u32[]{:S(2)}) copy-start(bf16[512,128]{0,1:T(8,128)(2,1)} %copy.323) | copy-start | bytes 393220
  209.7 3.9 copy-start.1
  211.3 3.8 copy-start.8
  295.5 4.8 copy-start.16
  300.2 4.0 copy-start.37
  351.9 14.8 %copy-start.6 = (f32[8,64,2,64]{3,1,2,0:T(8,128)S(1)}, f32[8,64,2,64]{3,1,2,0:T(8,128)}, u32[]{:S(2)}) copy-start(f32[8,64,2,64]{3,1,2,0:T(8,128)} %copy.312) | copy-start | bytes 786436
  351.9 14.8 %copy-start.12 = (f32[8,2,64,64]{3,0,1,2:T(8,128)S(1)}, f32[8,2,64,64]{3,0,1,2:T(8,128)}, u32[]{:S(2)}) copy-start(f32[8,2,64,64]{3,0,1,2:T(8,128)} %copy-done.11) | copy-start | bytes 786436
  373.5 13.8 %copy-start.47 = (s32[32,2]{0,1:T(2,128)S(1)}, s32[32,2]{0,1:T(2,128)}, u32[]{:S(2)}) copy-start(s32[32,2]{0,1:T(2,128)} %param.34) | copy-start | bytes 772
  373.5 14.4 %copy-start.46 = (bf16[2048]{0:T(1024)(128)(2,1)S(1)}, bf16[2048]{0:T(1024)(128)(2,1)}, u32[]{:S(2)}) copy-start(bf16[2048]{0:T(1024)(128)(2,1)} %param.33) | copy-start | bytes 12292
  373.5 23.1 %copy-start.38 = (bf16[32,2048]{1,0:T(8,128)(2,1)S(1)}, bf16[32,2048]{1,0:T(8,128)(2,1)}, u32[]{:S(2)}) copy-start(bf16[32,2048]{1,0:T(8,128)(2,1)} %param.24) | copy-start | bytes 393220
  378.8 17.9 %all-to-all-start.1 = ((bf16[8,2,32,128]{3,2,1,0:T(8,128)(2,1)}), bf16[8,2,32,128]{3,2,1,0:T(8,128)(2,1)S(1)}, u32[]{:S(2)}, u32[]{:S(2)}) async-start(bf16[8,2,32,128]{3,2,1,0:T(8,128)(2,1)} %copy.355), calls=%async_computation.1 | async-start | bytes 262144 | tf_op jit(solution)/shard_map/all_to_all | solution.py:78
  387.3 79.8 %all-gather.9.cloned.1.call-start = ((), (), s32[]{:S(2)}) async-start(), calls=%async_computation.6 | async-start | bytes 8912896 | tf_op jit(solution)/shard_map/all_gather | solution.py:266
  416.4 197.3 %reduce-scatter.2.cloned.1.call-start = ((), (), s32[]{:S(2)}) async-start(), calls=%async_computation.7 | async-start | bytes 8912896 | tf_op jit(solution)/shard_map/reduce_scatter | solution.py:288
  544.1 78.7 %copy-start.48 = (f32[32,2]{0,1:T(2,128)S(1)}, f32[32,2]{0,1:T(2,128)}, u32[]{:S(2)}) copy-start(f32[32,2]{0,1:T(2,128)} %param.35) | copy-start | bytes 772
  615.8 13.9 %all-to-all-start.3 = ((bf16[16,3,2,2048]{3,2,1,0:T(2,128)(2,1)}), bf16[16,3,2,2048]{3,2,1,0:T(2,128)(2,1)S(1)}, u32[]{:S(2)}, u32[]{:S(2)}) async-start(bf16[16,3,2,2048]{3,2,1,0:T(2,128)(2,1)} %reshape.426), calls=%async_computation.4 | async-start | bytes 786432 | tf_op jit(solution)/shard_map/all_to_all | solution.py:301
  (23 other events, 48.5 us)
Sparse Core Ops, SparseCore 0:
  9.2 58.8 all-gather.6
  416.5 50.5 all-gather.8
  544.3 69.4 reduce-scatter.1
where the time goes:
time: 651 us; the launch traced here: 639 us
  other arithmetic  191 us (29%)
  waiting for transfers between devices  136 us (21%)
  local copies, waits for them, and re-layouts  112 us (17%)
  matrix products  103 us (16%)
  blocking collectives  65.9 us (10%)
  starting transfers between devices  15.9 us (2%)
  between operations  14.8 us (2%)
    another operation x4, other arithmetic, block_terms(): jax.scipy.linalg.solve_triangular(triangle, right_side, lower=True, unit_...  160 us
    reduce_scatter x1, waiting for transfers between devices, body(): lax.psum_scatter(jnp.concatenate([routed_out, shared_out], axis=1).reshap...  69.6 us
    all_gather x1, waiting for transfers between devices, body(): everyone = lax.all_gather(own_block, TP, axis=0, tiled=True)  50.4 us
    all_gather x4, blocking collectives, gathered_once(): both, at, found = (lax.all_gather(jnp.concatenate(lines), axis), 0, {})  49 us
    dot_general x62, matrix products, chain_product(): jnp.einsum('...ij,...jk->...ik', left_mat, right_mat, precision=highest)  27.8 us
    dynamic_slice x32, local copies, waits for them, and re-layouts, block_chain(): lax.scan(advance, (identity, jnp.zeros_like(identity)), (transition, carr...  14.9 us
    all_to_all x1, blocking collectives, body(): lax.all_to_all(outgoing, SP, split_axis=0, concat_axis=0, tiled=True)  13 us
  transfers between devices with their start and end apart: 5, of which 4 were waited for; matrix products, arithmetic and copies ran while one was open for 49% of the time, Pallas kernels for 0%

commit v1 on v0

v1 whole, which is shorter than its diff:
```python
import functools

import jax
import jax.numpy as jnp
from jax import lax
from jax.experimental import pallas as pl
from jax.experimental.pallas import tpu as pltpu
from jax.sharding import PartitionSpec as P

SP = "sp"
TP = "tp"
BLOCK = 64
LANES = 128
GN_EPS = 0.00064
RMS_EPS = 1e-06
f32 = jnp.float32
bf16 = jnp.bfloat16
VMEM = pl.BlockSpec(memory_space=pltpu.VMEM)
NN = (((1,), (0,)), ((), ()))
NT = (((1,), (1,)), ((), ()))
TN = (((0,), (0,)), ((), ()))


def iota(shape, dim):
    return lax.broadcasted_iota(jnp.int32, shape, dim)


def halves(array):
    high = array.astype(bf16)
    return high, (array - high.astype(f32)).astype(bf16)


def raw_dot(left, right, dims):
    return lax.dot_general(left, right, dims, preferred_element_type=f32)


def both_heads(rows):
    lane = iota(rows.shape, 1)
    zero = jnp.zeros_like(rows)
    return jnp.concatenate(
        [jnp.where(lane < BLOCK, rows, zero), jnp.where(lane < BLOCK, zero, rows)], axis=0
    )


def fine_dot(left, right, dims, spread=False):
    left_high, left_low = halves(left)
    right_high, right_low = halves(right)
    if spread:
        right_high, right_low = both_heads(right_high), both_heads(right_low)
    if dims == TN:
        return raw_dot(
            jnp.concatenate([left_high, left_high, left_low], axis=0),
            jnp.concatenate([right_high, right_low, right_high], axis=0),
            TN,
        )
    count = left.shape[0]
    both = raw_dot(jnp.concatenate([left_high, left_low], axis=0), right_high, dims)
    return both[:count] + both[count:] + raw_dot(left_high, right_low, dims)


def exact_right_dot(left, right, dims):
    left_high, left_low = halves(left)
    count = left.shape[0]
    both = raw_dot(jnp.concatenate([left_high, left_low], axis=0), right, dims)
    return both[:count] + both[count:]


def head_sum(rows):
    ones = (iota((LANES, LANES), 0) // BLOCK == iota((LANES, LANES), 1) // BLOCK).astype(bf16)
    return exact_right_dot(rows, ones, NN)


def block_sums(log_decay):
    high = log_decay.astype(bf16)
    rest = log_decay - high.astype(f32)
    middle = rest.astype(bf16)
    low = (rest - middle.astype(f32)).astype(bf16)
    count = log_decay.shape[0]
    ones = (iota((count, count), 0) >= iota((count, count), 1)).astype(bf16)
    width = log_decay.shape[1]
    sums = raw_dot(ones, jnp.concatenate([high, middle, low], axis=1), NN)
    return sums[:, :width] + sums[:, width : 2 * width] + sums[:, 2 * width :]


def inverse(strict):
    row, lane = iota(strict.shape, 0), iota(strict.shape, 1) % BLOCK

    def within(size):
        return row // size == lane // size

    def product(left, right):
        return fine_dot(left, right, NN, spread=True)

    small = jnp.where(within(8), strict, 0.0)
    start = jnp.where(row == lane, 1.0, 0.0) - small
    square = product(small, small)
    both = product(jnp.concatenate([start, square], axis=0), square)
    result = start + both[:BLOCK]
    result = result + product(result, both[BLOCK:])
    for size in (8, 16, 32):
        edge = jnp.where(within(2 * size) & ~within(size), strict, 0.0)
        result = result - product(product(result, edge), result)
    return result


def one_way(unit, beta, key_rows, value_spread, read, left_unit, left_read, right, edge, lower):
    row, lane = iota((BLOCK, LANES), 0), iota((BLOCK, LANES), 1) % BLOCK
    strict = row > lane if lower else row < lane
    upto = row >= lane if lower else row <= lane
    unit_mid, read_mid = unit * left_unit, read * left_read
    beta_mid, key_mid = beta * right, key_rows * right
    left_high, left_low = halves(jnp.concatenate([unit_mid, read_mid], axis=0))
    beta_parts, key_parts = halves(beta_mid), halves(key_mid)
    right_high, right_low = [
        jnp.concatenate([both_heads(b), both_heads(k)], axis=0)
        for b, k in zip(beta_parts, key_parts)
    ]
    both = raw_dot(jnp.concatenate([left_high, left_low], axis=0), right_high, NT)
    pairs = both[: 2 * BLOCK] + both[2 * BLOCK :] + raw_dot(left_high, right_low, NT)
    erase_beta = jnp.where(strict, pairs[:BLOCK, :LANES], 0.0)
    erase_key = jnp.where(strict, pairs[:BLOCK, LANES:], 0.0)
    read_beta = jnp.where(upto, pairs[BLOCK:, :LANES], 0.0)
    read_key = jnp.where(upto, pairs[BLOCK:, LANES:], 0.0)
    keyed = exact_right_dot(jnp.concatenate([erase_key, read_key], axis=0), value_spread, NN)
    solver = inverse(erase_beta)
    lead = fine_dot(solver, unit_mid * edge, NN, spread=True)
    own = fine_dot(solver, -keyed[:BLOCK], NN, spread=True)
    solved = jnp.concatenate([lead, own], axis=1)
    parts = halves(solved)
    spread_parts = [
        jnp.concatenate([both_heads(p[:, :LANES]), both_heads(p[:, LANES:])], axis=1) for p in parts
    ]
    read_high, read_low = halves(read_beta)
    both = raw_dot(jnp.concatenate([read_high, read_low], axis=0), spread_parts[0], NN)
    applied = both[:BLOCK] + both[BLOCK:] + raw_dot(read_high, spread_parts[1], NN)
    readout = read_mid * edge - applied[:, :LANES]
    local = applied[:, LANES:] + keyed[BLOCK:]
    return solved, beta_mid * edge, key_mid * edge, readout, local


def mixer_kernel(
    read_ref,
    key_ref,
    value_ref,
    erase_ref,
    decay_ref,
    spike_ref,
    local_ref,
    readout_ref,
    prefix_ref,
    start_ref,
    whole_ref,
    move_ref,
    carry_ref,
    *,
    together,
):
    tokens = key_ref.shape[0]
    block_count = tokens // BLOCK
    lane = iota((BLOCK, LANES), 1)
    same_head = iota((LANES, LANES), 0) // BLOCK == iota((LANES, LANES), 1) // BLOCK
    diagonal = iota((LANES, LANES), 0) == iota((LANES, LANES), 1)

    def one_block(block):
        at = pl.ds(pl.multiple_of(block * BLOCK, BLOCK), BLOCK)
        key_rows = key_ref[at, :].astype(f32)
        read = read_ref[at, :].astype(f32)
        value = value_ref[at, :]
        unit = key_rows * lax.rsqrt(head_sum(key_rows * key_rows) + 1e-06)
        beta = unit * jax.nn.sigmoid(erase_ref[at, :].astype(f32))
        decay_in = decay_ref[at, :].astype(f32)
        spike = jnp.where(lane < BLOCK, spike_ref[at, 0:1], spike_ref[at, 1:2])
        log_decay = -jnp.exp(-jax.nn.softplus(-decay_in) - 0.5) + spike
        upto = block_sums(log_decay)
        total = upto[BLOCK - 1 :, :]
        middle = 0.5 * total
        ahead = upto - log_decay
        before, after = jnp.exp(ahead - middle), jnp.exp(upto - middle)
        until, since = jnp.exp(middle - upto), jnp.exp(middle - ahead)
        edge = jnp.exp(middle)
        value_spread = both_heads(value)
        ways = (
            one_way(unit, beta, key_rows, value_spread, read, before, after, until, edge, True),
            one_way(unit, beta, key_rows, value_spread, read, until, since, before, edge, False),
        )
        local_ref[at, :] = ways[0][4] + ways[1][4]
        over = jnp.exp(total)
        for way, (solved, beta_end, key_end, readout, _) in enumerate(ways):
            readout_ref[at, way * LANES : (way + 1) * LANES] = readout
            moved = fine_dot(solved, beta_end, TN)
            key_high, key_low = halves(key_end)
            keyed = raw_dot(
                jnp.concatenate([value, value], axis=0),
                jnp.concatenate([key_high, key_low], axis=0),
                TN,
            )
            move_ref[way, block] = jnp.where(
                same_head, jnp.where(diagonal, over, 0.0) - moved[:LANES], 0.0
            )
            carry = jnp.where(same_head, moved[LANES:] + keyed, 0.0)
            carry_ref[way, block] = carry[:BLOCK] + carry[BLOCK:]

    def step(index, _):
        for k in range(together):
            one_block(index * together + k)
        return 0

    lax.fori_loop(0, block_count // together, step, 0)
    identity = jnp.where(iota((BLOCK, LANES), 0) == iota((BLOCK, LANES), 1) % BLOCK, 1.0, 0.0)
    running = [jnp.concatenate([identity, jnp.zeros_like(identity)], axis=0)] * 2
    for k in range(block_count):
        for way in range(2):
            block = k if way == 0 else block_count - 1 - k
            now = running[way]
            prefix_ref[way, block] = now[:BLOCK]
            start_ref[way, block] = now[BLOCK:]
            after = fine_dot(now, move_ref[way, block], NN)
            running[way] = jnp.concatenate(
                [after[:BLOCK], after[BLOCK:] + carry_ref[way, block]], axis=0
            )
    for way in range(2):
        whole_ref[way] = running[way].astype(bf16)


def mixer_terms(read, keys, values, erase, decay, spike):
    tokens = keys.shape[0]
    block_count = tokens // BLOCK
    shape = jax.ShapeDtypeStruct
    return pl.pallas_call(
        functools.partial(mixer_kernel, together=2),
        name="mixer_terms",
        out_shape=(
            shape((tokens, LANES), f32),
            shape((tokens, 2 * LANES), f32),
            shape((2, block_count, BLOCK, LANES), f32),
            shape((2, block_count, BLOCK, LANES), f32),
            shape((2, 2 * BLOCK, LANES), bf16),
        ),
        in_specs=[VMEM] * 6,
        out_specs=[VMEM] * 5,
        scratch_shapes=[
            pltpu.VMEM((2, block_count, LANES, LANES), f32),
            pltpu.VMEM((2, block_count, BLOCK, LANES), f32),
        ],
    )(read, keys, values, erase, decay, spike)


def finish_kernel(place_ref, got_ref, local_ref, readout_ref, prefix_ref, start_ref, gain_ref, mixed_ref):
    place = place_ref[0]
    count = got_ref.shape[0]
    block_count = prefix_ref.shape[1]
    entry = [jnp.zeros((BLOCK, LANES), f32)] * 2
    for k in range(count - 1):
        for way in range(2):
            j = k if way == 0 else count - 1 - k
            passed = j < place if way == 0 else j > place
            moved = exact_right_dot(entry[way], both_heads(got_ref[j, :BLOCK, :]), NN)
            entry[way] = jnp.where(passed, moved + got_ref[j, BLOCK:, :].astype(f32), entry[way])
    entry_halves = [halves(e) for e in entry]
    gain = gain_ref[...].astype(f32)
    for block in range(block_count):
        parts = []
        for way in range(2):
            high, low = entry_halves[way]
            prefix = prefix_ref[way, block]
            prefix_high, prefix_low = [both_heads(p) for p in halves(prefix)]
            both = raw_dot(jnp.concatenate([high, low], axis=0), prefix_high, NN)
            state = both[:BLOCK] + both[BLOCK:] + raw_dot(high, prefix_low, NN)
            parts.append([both_heads(p) for p in halves(state + start_ref[way, block])])
        state_high, state_low = [jnp.concatenate([parts[0][k], parts[1][k]], axis=1) for k in (0, 1)]
        at = slice(block * BLOCK, (block + 1) * BLOCK)
        read_high, read_low = halves(readout_ref[at, :])
        both = raw_dot(jnp.concatenate([read_high, read_low], axis=0), state_high, NT)
        mix = local_ref[at, :] + both[:BLOCK] + both[BLOCK:] + raw_dot(read_high, state_low, NT)
        center = mix - head_sum(mix) * (1.0 / BLOCK)
        spread = head_sum(center * center) * (1.0 / BLOCK)
        mixed_ref[at, :] = (center * lax.rsqrt(spread + GN_EPS) * gain).astype(bf16)


def finish_mix(place, got, local, readout, prefix, start, gain):
    return pl.pallas_call(
        finish_kernel,
        name="finish_mix",
        out_shape=jax.ShapeDtypeStruct(local.shape, bf16),
        in_specs=[pl.BlockSpec(memory_space=pltpu.SMEM)] + [VMEM] * 6,
        out_specs=VMEM,
    )(place, got, local, readout, prefix, start, gain)


def push_kernel(x_ref, o_ref, send_sem, recv_sem, *, axis, count, source, target):
    me = lax.axis_index(axis)
    barrier = pltpu.get_barrier_semaphore()
    for k in range(1, count):
        pl.semaphore_signal(barrier, inc=1, device_id={axis: lax.rem(me + k, count)})
    pl.semaphore_wait(barrier, count - 1)
    copies = []
    for k in range(1, count):
        peer = lax.rem(me + k, count)
        copy = pltpu.make_async_remote_copy(
            src_ref=source(x_ref, me, peer, count),
            dst_ref=target(o_ref, me),
            send_sem=send_sem.at[k],
            recv_sem=recv_sem.at[k],
            device_id={axis: peer},
        )
        copy.start()
        copies.append(copy)
    target(o_ref, me)[...] = source(x_ref, me, me, count)[...]
    for copy in copies:
        copy.wait()


def push(x, out_shape, axis, count, source, target, number, name):
    return pl.pallas_call(
        functools.partial(push_kernel, axis=axis, count=count, source=source, target=target),
        name=name,
        out_shape=jax.ShapeDtypeStruct(out_shape, x.dtype),
        in_specs=[VMEM],
        out_specs=VMEM,
        scratch_shapes=[pltpu.SemaphoreType.DMA((count,)), pltpu.SemaphoreType.DMA((count,))],
        compiler_params=pltpu.CompilerParams(collective_id=number, has_side_effects=True),
    )(x)


def way_for(x_ref, me, peer, count):
    return x_ref.at[(me + count - peer) // (count + 1)]


def slot_of_peer(x_ref, me, peer, count):
    return x_ref.at[peer]


def at_slot(o_ref, me):
    return o_ref.at[me]


def at_lanes(o_ref, me):
    return o_ref.at[:, pl.ds(pl.multiple_of(me * LANES, LANES), LANES)]


def expert_kernel(x_ref, gate_ref, up_ref, down_ref, *rest):
    o_ref = rest[-1]
    groups, rows, width = x_ref.shape
    x = x_ref[...].reshape(groups * rows, width)
    gate = raw_dot(x, gate_ref[0], NN)
    up = raw_dot(x, up_ref[0], NN)
    hidden = (gate / (1.0 + jnp.exp(-gate)) * up).astype(bf16)
    o_ref[...] = raw_dot(hidden, down_ref[0], NN).astype(bf16).reshape(groups, rows, width)


def expert_rows(slab, gate, up, down, rows, first, into, name):
    groups, _, width = slab.shape
    steps, _, hidden = gate.shape
    specs = [
        pl.BlockSpec((groups, rows, width), lambda e: (0, first + e, 0)),
        pl.BlockSpec((1, width, hidden), lambda e: (e, 0, 0)),
        pl.BlockSpec((1, width, hidden), lambda e: (e, 0, 0)),
        pl.BlockSpec((1, hidden, width), lambda e: (e, 0, 0)),
    ]
    arrays = [slab, gate, up, down]
    aliases = {}
    if into is not None:
        specs.append(pl.BlockSpec(memory_space=pl.ANY))
        arrays.append(into)
        aliases = {4: 0}
    return pl.pallas_call(
        expert_kernel,
        name=name,
        grid=(steps,),
        out_shape=jax.ShapeDtypeStruct(slab.shape, bf16),
        in_specs=specs,
        out_specs=pl.BlockSpec((groups, rows, width), lambda e: (0, first + e, 0)),
        input_output_aliases=aliases,
        compiler_params=pltpu.CompilerParams(vmem_limit_bytes=56 * 1024 * 1024),
    )(*arrays)


def body(
    layer_input,
    receptance,
    keys,
    values,
    erase_preact,
    decay_preact,
    decay_spike,
    head_norm_gain,
    output_weight,
    expert_norm_gain,
    routes,
    routing_weight,
    expert_gate_weight,
    expert_up_weight,
    expert_down_weight,
    shared_gate_weight,
    shared_up_weight,
    shared_down_weight,
):
    sp_count, tp_count = lax.axis_size(SP), lax.axis_size(TP)
    local, readout, prefix, start, whole = mixer_terms(
        receptance, keys, values, erase_preact, decay_preact, decay_spike
    )
    got = push(whole, (sp_count,) + whole.shape[1:], SP, sp_count, way_for, at_slot, 0, "states")
    place = lax.axis_index(SP).astype(jnp.int32).reshape(1)
    mixed = finish_mix(place, got, local, readout, prefix, start, head_norm_gain.reshape(1, -1))
    row_count, model_width = layer_input.shape
    token_major = push(
        mixed.reshape(tp_count, row_count, LANES),
        (row_count, model_width),
        TP,
        tp_count,
        slot_of_peer,
        at_lanes,
        1,
        "heads",
    )
    projected = jnp.dot(
        token_major,
        lax.all_gather(output_weight, TP, axis=0, tiled=True),
        preferred_element_type=f32,
    )
    residual = layer_input.astype(f32) + projected
    normed = residual * lax.rsqrt(jnp.mean(residual * residual, axis=-1, keepdims=True) + RMS_EPS)
    normed = (normed * expert_norm_gain.astype(f32)).astype(bf16)

    top_count = routes.shape[1]
    expert_local = expert_gate_weight.shape[0]
    capacity = 3
    room = 8
    slot_total = sp_count * room
    entries = routes.reshape(-1)
    entry_count = entries.shape[0]
    expert_hot = (entries[:, None] == jnp.arange(expert_local * sp_count)[None, :]).astype(jnp.int32)
    rank_in = jnp.sum((jnp.cumsum(expert_hot, axis=0) - 1) * expert_hot, axis=1)
    slot_of = entries // expert_local * room + entries % expert_local * capacity + rank_in
    slot_hot = slot_of[:, None] == jnp.arange(slot_total)[None, :]
    placing = jnp.sum(
        slot_hot.reshape(row_count, top_count, slot_total).astype(f32), axis=1
    ).astype(bf16)
    weighting = jnp.sum(
        jnp.where(slot_hot, routing_weight.reshape(-1, 1), 0.0).reshape(
            row_count, top_count, slot_total
        ),
        axis=1,
    )
    outgoing = lax.dot_general(placing, normed, TN, preferred_element_type=f32).astype(bf16)
    arrived = push(
        outgoing.reshape(sp_count, room, model_width),
        (sp_count, room, model_width),
        SP,
        sp_count,
        slot_of_peer,
        at_slot,
        2,
        "to_experts",
    ).reshape(slot_total, model_width)
    used = sp_count * capacity
    packed_row = jnp.arange(expert_local * used)
    from_slot = (
        packed_row % used // capacity * room
        + packed_row // used * capacity
        + packed_row % capacity
    )
    packing = (from_slot[:, None] == jnp.arange(slot_total)[None, :]).astype(bf16)
    packed = jnp.dot(packing, arrived, preferred_element_type=f32).astype(bf16)
    own_block = jnp.concatenate([packed, normed], axis=0)
    block_rows = own_block.shape[0]
    slab = lax.all_gather(own_block, TP, axis=0, tiled=True)
    slab = slab.reshape(tp_count, block_rows, model_width)
    outs = expert_rows(
        slab, expert_gate_weight, expert_up_weight, expert_down_weight, used, 0, None, "routed"
    )
    outs = expert_rows(
        slab,
        shared_gate_weight[None],
        shared_up_weight[None],
        shared_down_weight[None],
        row_count,
        expert_local * used // row_count,
        outs,
        "shared",
    )
    summed = lax.psum_scatter(
        outs.reshape(tp_count * block_rows, model_width), TP, scatter_dimension=0, tiled=True
    )
    unpacked = lax.dot_general(
        packing, summed[: expert_local * used], TN, preferred_element_type=f32
    ).astype(bf16)
    returned = push(
        unpacked.reshape(sp_count, room, model_width),
        (sp_count, room, model_width),
        SP,
        sp_count,
        slot_of_peer,
        at_slot,
        3,
        "to_tokens",
    ).reshape(slot_total, model_width)
    weight_high, weight_rest = halves(weighting)
    routed = jnp.dot(weight_high, returned, preferred_element_type=f32) + jnp.dot(
        weight_rest, returned, preferred_element_type=f32
    )
    return (residual + summed[expert_local * used :].astype(f32) + routed).astype(bf16)


def solution(mesh):
    both = (SP, TP)
    in_specs = (
        P(both, None),
        P(SP, TP),
        P(SP, TP),
        P(SP, TP),
        P(SP, TP),
        P(SP, TP),
        P(SP, TP),
        P(TP),
        P(TP, None),
        P(),
        P(both, None),
        P(both, None),
        P(SP, None, TP),
        P(SP, None, TP),
        P(SP, TP, None),
        P(None, TP),
        P(None, TP),
        P(TP, None),
    )
    return jax.shard_map(
        body, mesh=mesh, in_specs=in_specs, out_specs=P(both, None), check_vma=False
    )
```

time: 651 us -> 270 us (0.41); the launches traced: 639 us -> 269 us
  other arithmetic: 191 us -> 2.84 us
  Pallas kernels: 0 us -> 112 us
  local copies, waits for them, and re-layouts: 112 us -> 2.6 us
  matrix products: 103 us -> 12.9 us
  blocking collectives: 65.9 us -> 0 us
  starting transfers between devices: 15.9 us -> 0.26 us
  waiting for transfers between devices: 136 us -> 125 us
    another operation x6 -> x0, other arithmetic: 161 us -> none  [the longest x4 160 us: block_terms(): jax.scipy.linalg.solve_triangular(triangle, right_side, lower=True, unit_...]
    pallas_call x0 -> x8, Pallas kernels: none -> 112 us  [the longest x4 55.1 us: push(): pl.pallas_call(functools.partial(push_kernel, axis=axis, count=count, sou...]
    dot_general x96 -> x5, matrix products: 92.3 us -> 7.87 us  [the longest x1 2.22 us: body(): lax.dot_general(packing, summed[:expert_local * used], TN, preferred_elem...]
    all_gather x4 -> x0, blocking collectives: 49 us -> none  [gathered_once(): both, at, found = (lax.all_gather(jnp.concatenate(lines), axis), 0, {})]
    reshape x27 -> x0, local copies, waits for them, and re-layouts: 34.6 us -> none  [the longest x1 10.9 us: body(): routed_in = slab[:, :slot_total].reshape(-1, expert_local, model_width)]
    all_to_all x2 -> x0, blocking collectives: 16.9 us -> none  [the longest x1 13 us: body(): lax.all_to_all(outgoing, SP, split_axis=0, concat_axis=0, tiled=True)]
    all_to_all x2 -> x0, starting transfers between devices: 15.6 us -> none  [the longest x1 8.5 us: turned_blocks(): whole = lax.all_to_all(whole, axes[k], k, k, tiled=True)]
    transpose x3 -> x0, local copies, waits for them, and re-layouts: 15 us -> none  [the longest x1 12.6 us: body(): jnp.einsum('rjh,jhd->rjd', hidden, expert_down_weight, preferred_element_...]
  transfers between devices with their start and end apart: 5 -> 3, of which waited for: 4 -> 2; matrix products, arithmetic and copies ran while one was open for 49% -> 2% of each run, Pallas kernels for 0% -> 26%
where the time goes in v1:
time: 270 us; the launch traced here: 269 us
  waiting for transfers between devices  125 us (46%)
  Pallas kernels  112 us (41%)
  between operations  13.2 us (5%)
  matrix products  12.9 us (5%)
  other arithmetic  2.84 us (1%)
    reduce_scatter x1, waiting for transfers between devices, body(): lax.psum_scatter(outs.reshape(tp_count * block_rows, model_width), TP, sc...  69.3 us
    all_gather x1, waiting for transfers between devices, body(): slab = lax.all_gather(own_block, TP, axis=0, tiled=True)  55.3 us
    pallas_call x4, Pallas kernels, push(): pl.pallas_call(functools.partial(push_kernel, axis=axis, count=count, sou...  55.1 us
    pallas_call x1, Pallas kernels, mixer_terms(): pl.pallas_call(functools.partial(mixer_kernel, together=2), name='mixer_t...  33.2 us
    pallas_call x2, Pallas kernels, expert_rows(): pl.pallas_call(expert_kernel, name=name, grid=(steps,), out_shape=jax.Sha...  15.3 us
    pallas_call x1, Pallas kernels, finish_mix(): pl.pallas_call(finish_kernel, name='finish_mix', out_shape=jax.ShapeDtype...  8.41 us
  transfers between devices with their start and end apart: 3, of which 2 were waited for; matrix products, arithmetic and copies ran while one was open for 2% of the time, Pallas kernels for 26%

profile of v1, /device:TPU:6, one launch (start us, length us, event | category | flops | bytes accessed | tf_op | source)
XLA Modules:
  0.0 269.4 jit_solution(6580422464747676878)
XLA Ops:
  6.5 0.7 all-gather.3.cloned.1.call-update
  7.3 0.0 all-gather.5.cloned.1.call-start
  7.3 0.7 convert_element_type.47
  8.0 0.8 copy.35
  8.8 0.1 eq.57
  8.9 0.1 fusion.9
  8.9 0.1 reduce_window_sum.11
  9.0 0.2 select_reduce_fusion.1
  9.2 0.1 reduce_sum.39
  9.4 0.1 copy.40
  9.4 1.6 copy.34.spike_ref
  11.0 33.2 %mixer_terms.1 = (f32[512,128]{1,0:T(8,128)}, f32[512,256]{1,0:T(8,128)}, f32[2,8,64,128]{3,2,1,0:T(8,128)}, f32[2,8,64,128]{3,2,1,0:T(8,128)}, bf16[2,128,128]{2,1,0:T(8,128)(2,1)}) custom-call(bf16[512,128]{1,0:T(8,128)(2,1)} %read_ref.1, bf16[512,128]{1,0:T(8,128)(2,1)} %key_ref.1, bf16[512,128]{1,0:T(8,128)(2,1)} %value_ref.1, ...), custom_call_target="tpu_custom_call" | custom-call | tf_op jit(solution)/shard_map/mixer_terms/pallas_call | solution.py:229
  44.2 14.4 %states.1.got_ref = bf16[16,128,128]{2,1,0:T(8,128)(2,1)} custom-call(bf16[2,128,128]{2,1,0:T(8,128)(2,1)} %get-tuple-element.10.x_ref), custom_call_target="tpu_custom_call" | custom-call | tf_op jit(solution)/shard_map/states/pallas_call | solution.py:314
  58.6 8.4 %finish_mix.1 = bf16[512,128]{1,0:T(8,128)(2,1)} custom-call(s32[1]{0:T(128)} %bitcast.place_ref, bf16[16,128,128]{2,1,0:T(8,128)(2,1)} %states.1.got_ref, f32[512,128]{1,0:T(8,128)} %get-tuple-element.11.local_ref, f32[512,256]{1,0:T(8,128)} %get-tuple-element.12.readout_ref, f32[2,8,64,128]{3,2,1,0:T(8,128)} %get-tuple-element.13.prefix_ref, ...), custom_call_target="tpu_custom_call" | custom-call | tf_op jit(solution)/shard_map/finish_mix/pallas_call | solution.py:281
  67.0 13.6 %heads.1 = bf16[32,2048]{1,0:T(8,128)(2,1)} custom-call(bf16[16,32,128]{2,1,0:T(8,128)(2,1)} %bitcast.30), custom_call_target="tpu_custom_call" | custom-call | tf_op jit(solution)/shard_map/heads/pallas_call | solution.py:314
  80.6 0.8 select_reduce_fusion
  81.4 0.0 all-gather.3.cloned.1.call-done
  81.4 5.0 %multiply_reduce_fusion = (f32[32]{0:T(128)S(1)}, f32[32,2048]{1,0:T(8,128)S(1)}) fusion(bf16[32,2048]{1,0:T(8,128)(2,1)} %heads.1, bf16[2048,2048]{1,0:T(8,128)(2,1)} %all-gather.3.cloned.1.call-done, bf16[32,2048]{1,0:T(8,128)(2,1)} %param.18), kind=kOutput, calls=%fused_computation.16 | convolution fusion | flops 268697568 | bytes 8913024 | tf_op jit(solution)/shard_map/dot_general | solution.py:416
  86.5 0.1 multiply_convert_fusion
  86.6 1.1 fusion.x_ref
  87.7 14.7 %to_experts.1 = bf16[16,8,2048]{2,1,0:T(8,128)(2,1)} custom-call(bf16[16,8,2048]{2,1,0:T(8,128)(2,1)} %fusion.x_ref), custom_call_target="tpu_custom_call" | custom-call | tf_op jit(solution)/shard_map/to_experts/pallas_call | solution.py:314
  102.4 1.4 convolution_convert_fusion.2
  103.8 0.9 pad_maximum_fusion
  104.7 0.2 reduce-scatter.2.cloned.1.call-start
  104.9 55.3 %all-gather.5.cloned.1.call-done = bf16[2048,2048]{1,0:T(8,128)(2,1)} async-done(((bf16[128,2048]{1,0:T(8,128)(2,1)}), bf16[2048,2048]{1,0:T(8,128)(2,1)}) %all-gather.5.cloned.1.call-update) | async-done | bytes 8388624 | tf_op jit(solution)/shard_map/all_gather | solution.py:467
  160.2 9.7 %routed.1.rest_0_ = bf16[16,128,2048]{2,1,0:T(8,128)(2,1)} custom-call(bf16[16,128,2048]{2,1,0:T(8,128)(2,1)} %bitcast.25, bf16[2,2048,256]{2,1,0:T(8,128)(2,1)} %gate_ref.1, bf16[2,2048,256]{2,1,0:T(8,128)(2,1)} %up_ref.1, bf16[2,256,2048]{2,1,0:T(8,128)(2,1)} %down_ref.1), custom_call_target="tpu_custom_call" | custom-call | tf_op jit(solution)/shard_map/routed/pallas_call | solution.py:366
  169.9 5.6 %shared.1 = bf16[16,128,2048]{2,1,0:T(8,128)(2,1)} custom-call(bf16[16,128,2048]{2,1,0:T(8,128)(2,1)} %bitcast.26, bf16[1,2048,256]{2,1,0:T(8,128)(2,1)} %bitcast.27, bf16[1,2048,256]{2,1,0:T(8,128)(2,1)} %bitcast.28, bf16[1,256,2048]{2,1,0:T(8,128)(2,1)} %bitcast.29, bf16[16,128,2048]{2,1,0:T(8,128)(2,1)} %routed.1.rest_0_), custom_call_target="tpu_custom_call", output_to_operand_aliasing={{}: (4, {})} | custom-call | tf_op jit(solution)/shard_map/shared/pallas_call | solution.py:366
  175.6 69.3 %reduce-scatter.2.cloned.1.call-done = bf16[128,2048]{1,0:T(8,128)(2,1)} async-done(((bf16[2048,2048]{1,0:T(8,128)(2,1)}), bf16[128,2048]{1,0:T(8,128)(2,1)}) %reduce-scatter.2.cloned.1.call-update) | async-done | bytes 524304 | tf_op jit(solution)/shard_map/reduce_scatter | solution.py:482
  244.9 2.2 fusion.1.x_ref
  247.2 12.5 %to_tokens.1 = bf16[16,8,2048]{2,1,0:T(8,128)(2,1)} custom-call(bf16[16,8,2048]{2,1,0:T(8,128)(2,1)} %fusion.1.x_ref), custom_call_target="tpu_custom_call" | custom-call | tf_op jit(solution)/shard_map/to_tokens/pallas_call | solution.py:314
  259.7 1.2 fusion.5
  260.9 1.9 fusion.3
  (6 shorter events, 0.1 us)
Async XLA Ops:
  6.5 74.9 %all-gather.3.cloned.1.call-start = ((), (), s32[]{:S(2)}) async-start(), calls=%async_computation.1 | async-start | bytes 8912896 | tf_op jit(solution)/shard_map/all_gather | solution.py:418
  7.3 153.0 %all-gather.5.cloned.1.call-start = ((), (), s32[]{:S(2)}) async-start(), calls=%async_computation.2 | async-start | bytes 8912896 | tf_op jit(solution)/shard_map/all_gather | solution.py:467
  104.7 140.3 %reduce-scatter.2.cloned.1.call-start = ((), (), s32[]{:S(2)}) async-start(), calls=%async_computation.3 | async-start | bytes 8912896 | tf_op jit(solution)/shard_map/reduce_scatter | solution.py:482
Sparse Core Ops, SparseCore 0:
  9.2 58.8 all-gather.2
  104.8 55.3 all-gather.4
  175.7 69.1 reduce-scatter.1

commit v2 on v1

--- a/solution.py
+++ b/solution.py
@@ -338,41 +338,273 @@
     return o_ref.at[:, pl.ds(pl.multiple_of(me * LANES, LANES), LANES)]
 
 
-def expert_kernel(x_ref, gate_ref, up_ref, down_ref, *rest):
-    o_ref = rest[-1]
-    groups, rows, width = x_ref.shape
-    x = x_ref[...].reshape(groups * rows, width)
-    gate = raw_dot(x, gate_ref[0], NN)
-    up = raw_dot(x, up_ref[0], NN)
-    hidden = (gate / (1.0 + jnp.exp(-gate)) * up).astype(bf16)
-    o_ref[...] = raw_dot(hidden, down_ref[0], NN).astype(bf16).reshape(groups, rows, width)
-
-
-def expert_rows(slab, gate, up, down, rows, first, into, name):
-    groups, _, width = slab.shape
-    steps, _, hidden = gate.shape
-    specs = [
-        pl.BlockSpec((groups, rows, width), lambda e: (0, first + e, 0)),
-        pl.BlockSpec((1, width, hidden), lambda e: (e, 0, 0)),
-        pl.BlockSpec((1, width, hidden), lambda e: (e, 0, 0)),
-        pl.BlockSpec((1, hidden, width), lambda e: (e, 0, 0)),
-    ]
-    arrays = [slab, gate, up, down]
-    aliases = {}
-    if into is not None:
-        specs.append(pl.BlockSpec(memory_space=pl.ANY))
-        arrays.append(into)
-        aliases = {4: 0}
+def ring_kernel(
+    x_ref,
+    expert_gate,
+    expert_up,
+    expert_down,
+    shared_gate,
+    shared_up,
+    shared_down,
+    o_ref,
+    blocks,
+    partial,
+    other,
+    right_in,
+    left_in,
+    gate,
+    up,
+    down,
+    weight_sem,
+    gather_send,
+    gather_recv,
+    pass_send,
+    pass_recv,
+    pair_send,
+    pair_recv,
+    sum_send,
+    sum_recv,
+    *,
+    axis,
+    chips,
+    used,
+):
+    me = lax.axis_index(axis)
+    chip, core = me // 2, lax.rem(me, 2)
+    rows, width = x_ref.shape
+    half = rows // 2
+    far = chips // 2
+    steps = chips - 1
+    local_experts = expert_gate.shape[0]
+    hidden = shared_gate.shape[1]
+    ways = ((1, 0), (-1, 1))
+
+    def chip_at(distance):
+        return lax.rem(chip + distance + chips, chips)
+
+    def slot(distance, which):
+        return chip_at(distance) * 2 + which
+
+    ahead, behind, twin = slot(1, core), slot(-1, core), chip * 2 + 1 - core
+
+    weight_copies = []
+    for k, (pair, single, into) in enumerate(
+        ((expert_gate, shared_gate, gate), (expert_up, shared_up, up), (expert_down, shared_down, down))
+    ):
+        weight_copies.append(
+            pltpu.make_async_copy(pair, into.at[pl.ds(0, local_experts)], weight_sem.at[2 * k])
+        )
+        weight_copies.append(
+            pltpu.make_async_copy(single, into.at[local_experts], weight_sem.at[2 * k + 1])
+        )
+    for copy in weight_copies:
+        copy.start()
+
+    barrier = pltpu.get_barrier_semaphore()
+    for peer in (ahead, behind, twin):
+        pl.semaphore_signal(barrier, inc=1, device_id={axis: peer})
+    pl.semaphore_wait(barrier, 3)
+
+    def part(which):
+        return pl.ds(which * half, half)
+
+    def half_of(way, step):
+        return step % 2 if way == 0 else 1 - step % 2
+
+    def remote(source, target, send, recv, peer):
+        return pltpu.make_async_remote_copy(
+            src_ref=source, dst_ref=target, send_sem=send, recv_sem=recv, device_id={axis: peer}
+        )
+
+    sent = []
+
+    def start(copy):
+        copy.start()
+        sent.append(copy)
+
+    def gather_copy(way, step):
+        sign = ways[way][0]
+        at = slot(-sign * (step // 2), core)
+        piece = part(half_of(way, step))
+        source = x_ref.at[piece] if step < 2 else blocks.at[at, piece]
+        return remote(
+            source,
+            blocks.at[at, piece],
+            gather_send.at[way, step],
+            gather_recv.at[way, step],
+            ahead if way == 0 else behind,
+        )
+
+    def pass_copy(way, step):
+        sign = ways[way][0]
+        at = slot(-sign * (step // 2 + 1), core)
+        piece = part(half_of(way, step))
+        return remote(
+            blocks.at[at, piece],
+            blocks.at[at, piece],
+            pass_send.at[way, step],
+            pass_recv.at[way, step],
+            twin,
+        )
+
+    own_copy = remote(
+        x_ref, blocks.at[me], pass_send.at[0, steps], pass_recv.at[0, steps], twin
+    )
+    for step in (0, 1):
+        for way in (0, 1):
+            start(gather_copy(way, step))
+    start(own_copy)
+    blocks[me] = x_ref[...]
+
+    def experts_on(distance):
+        first = chip_at(distance) * 2
+
+        def one(k, _):
+            which = lax.rem(k + local_experts, local_experts + 1)
+            begin = pl.multiple_of(
+                used * (k // 2) + (rows - used) * ((2 - k) // 2), 16
+            )
+            at = pl.ds(begin, used)
+            x = blocks[pl.ds(first, 2), at, :].reshape(2 * used, width)
+            gated = raw_dot(x, gate[which], NN)
+            lifted = raw_dot(x, up[which], NN)
+            inner = (gated / (1.0 + jnp.exp(-gated)) * lifted).astype(bf16)
+            partial[pl.ds(first, 2), at, :] = (
+                raw_dot(inner, down[which], NN).astype(bf16).reshape(2, used, width)
+            )
+            return 0
+
+        lax.fori_loop(0, local_experts + 1, one, 0)
+
+    def pair_copy(distance):
+        at = slot(distance, 1 - core)
+        index = chip_at(distance)
+        return remote(
+            partial.at[at], other.at[index], pair_send.at[index], pair_recv.at[index], twin
+        )
+
+    for copy in weight_copies:
+        copy.wait()
+    own_copy.wait_recv()
+    experts_on(0)
+    waiting = [0]
+    for step in range(steps):
+        for way in (0, 1):
+            gather_copy(way, step).wait_recv()
+            if step + 2 < steps:
+                start(gather_copy(way, step + 2))
+            start(pass_copy(way, step))
+        for distance in waiting:
+            start(pair_copy(distance))
+        waiting = []
+        if step % 2 == 1:
+            for way in (0, 1):
+                for s in (step - 1, step):
+                    pass_copy(way, s).wait_recv()
+            distance = (step + 1) // 2
+
+            def both(k, _):
+                experts_on(distance * (2 * k - 1))
+                return 0
+
+            lax.fori_loop(0, 2, both, 0)
+            waiting = [-distance, distance]
+    for way in (0, 1):
+        pass_copy(way, steps - 1).wait_recv()
+    experts_on(far)
+    for distance in (far,):
+        start(pair_copy(distance))
+
+    def sum_distance(step):
+        return far - (step + 1) // 2
+
+    inbox = (right_in, left_in)
+
+    def sum_copy(way, step):
+        sign = ways[way][0]
+        at = slot(sign * sum_distance(step), core)
+        return remote(
+            partial.at[at, part(sum_half_of(way, step))],
+            inbox[way].at[step],
+            sum_send.at[way, step],
+            sum_recv.at[way, step],
+            ahead if way == 0 else behind,
+        )
+
+    def sum_half_of(way, step):
+        return step % 2 if way == 0 else 1 - step % 2
+
+    met = set()
+
+    def meet(distance):
+        key = distance % chips
+        if key not in met:
+            met.add(key)
+            pair_copy(distance).wait_recv()
+
+    for step in range(steps):
+        for way in (0, 1):
+            sign = ways[way][0]
+            distance = sign * sum_distance(step)
+            meet(distance)
+            at, piece = slot(distance, core), part(sum_half_of(way, step))
+            total = partial[at, piece, :].astype(f32) + other[chip_at(distance), piece, :].astype(f32)
+            if step >= 2:
+                sum_copy(way, step - 2).wait_recv()
+                total = total + inbox[way][step - 2].astype(f32)
+            partial[at, piece, :] = total.astype(bf16)
+        for way in (0, 1):
+            start(sum_copy(way, step))
+    meet(0)
+    for which in (0, 1):
+        piece = part(which)
+        total = partial[me, piece, :].astype(f32) + other[chip, piece, :].astype(f32)
+        for way in (0, 1):
+            step = steps - 2 if sum_half_of(way, steps - 2) == which else steps - 1
+            sum_copy(way, step).wait_recv()
+            total = total + inbox[way][step].astype(f32)
+        o_ref[piece, :] = total.astype(bf16)
+    for copy in sent:
+        copy.wait_send()
+
+
+def experts_over(x, weights, axis, devices, used, number, name):
+    rows, width = x.shape
+    hidden = weights[3].shape[1]
+    local_experts = weights[0].shape[0]
+    chips = devices // 2
+    steps = chips - 1
+    dma = pltpu.SemaphoreType.DMA
+    anywhere = pl.BlockSpec(memory_space=pl.ANY)
     return pl.pallas_call(
-        expert_kernel,
+        functools.partial(ring_kernel, axis=axis, chips=chips, used=used),
         name=name,
-        grid=(steps,),
-        out_shape=jax.ShapeDtypeStruct(slab.shape, bf16),
-        in_specs=specs,
-        out_specs=pl.BlockSpec((groups, rows, width), lambda e: (0, first + e, 0)),
-        input_output_aliases=aliases,
-        compiler_params=pltpu.CompilerParams(vmem_limit_bytes=56 * 1024 * 1024),
-    )(*arrays)
+        out_shape=jax.ShapeDtypeStruct((rows, width), bf16),
+        in_specs=[VMEM] + [anywhere] * 6,
+        out_specs=VMEM,
+        scratch_shapes=[
+            pltpu.VMEM((devices, rows, width), bf16),
+            pltpu.VMEM((devices, rows, width), bf16),
+            pltpu.VMEM((chips, rows, width), bf16),
+            pltpu.VMEM((steps, rows // 2, width), bf16),
+            pltpu.VMEM((steps, rows // 2, width), bf16),
+            pltpu.VMEM((local_experts + 1, width, hidden), bf16),
+            pltpu.VMEM((local_experts + 1, width, hidden), bf16),
+            pltpu.VMEM((local_experts + 1, hidden, width), bf16),
+            dma((6,)),
+            dma((2, steps)),
+            dma((2, steps)),
+            dma((2, steps + 1)),
+            dma((2, steps + 1)),
+            dma((chips,)),
+            dma((chips,)),
+            dma((2, steps)),
+            dma((2, steps)),
+        ],
+        compiler_params=pltpu.CompilerParams(
+            collective_id=number, has_side_effects=True, vmem_limit_bytes=58 * 1024 * 1024
+        ),
+    )(x, *weights)
 
 
 def body(
@@ -463,24 +695,21 @@
     packing = (from_slot[:, None] == jnp.arange(slot_total)[None, :]).astype(bf16)
     packed = jnp.dot(packing, arrived, preferred_element_type=f32).astype(bf16)
     own_block = jnp.concatenate([packed, normed], axis=0)
-    block_rows = own_block.shape[0]
-    slab = lax.all_gather(own_block, TP, axis=0, tiled=True)
-    slab = slab.reshape(tp_count, block_rows, model_width)
-    outs = expert_rows(
-        slab, expert_gate_weight, expert_up_weight, expert_down_weight, used, 0, None, "routed"
-    )
-    outs = expert_rows(
-        slab,
-        shared_gate_weight[None],
-        shared_up_weight[None],
-        shared_down_weight[None],
-        row_count,
-        expert_local * used // row_count,
-        outs,
-        "shared",
-    )
-    summed = lax.psum_scatter(
-        outs.reshape(tp_count * block_rows, model_width), TP, scatter_dimension=0, tiled=True
+    summed = experts_over(
+        own_block,
+        (
+            expert_gate_weight,
+            expert_up_weight,
+            expert_down_weight,
+            shared_gate_weight,
+            shared_up_weight,
+            shared_down_weight,
+        ),
+        TP,
+        tp_count,
+        used,
+        4,
+        "experts",
     )
     unpacked = lax.dot_general(
         packing, summed[: expert_local * used], TN, preferred_element_type=f32

time: 270 us -> 227 us (0.84)
  waiting for transfers between devices: 125 us -> 0.73 us
  Pallas kernels: 112 us -> 193 us
    pallas_call x2 -> x1, Pallas kernels: 15.3 us -> 94.1 us  [experts_over(): pl.pallas_call(functools.partial(ring_kernel, axis=axis, chips=chips, use...]
    reduce_scatter x1 -> x0, waiting for transfers between devices: 69.3 us -> none  [body(): lax.psum_scatter(outs.reshape(tp_count * block_rows, model_width), TP, sc...]
    all_gather x1 -> x0, waiting for transfers between devices: 55.3 us -> none  [body(): slab = lax.all_gather(own_block, TP, axis=0, tiled=True)]
  transfers between devices with their start and end apart: 3 -> 1, of which waited for: 2 -> 0; matrix products, arithmetic and copies ran while one was open for 2% -> 2% of each run, Pallas kernels for 26% -> 31%
where the time goes in v2:
time: 227 us; the launch traced here: 226 us
  Pallas kernels  193 us (85%)
  between operations  13.5 us (6%)
  matrix products  12.9 us (6%)
  other arithmetic  2.81 us (1%)
  local copies, waits for them, and re-layouts  2.6 us (1%)
    pallas_call x1, Pallas kernels, experts_over(): pl.pallas_call(functools.partial(ring_kernel, axis=axis, chips=chips, use...  94.1 us
    pallas_call x4, Pallas kernels, push(): pl.pallas_call(functools.partial(push_kernel, axis=axis, count=count, sou...  57.3 us
    pallas_call x1, Pallas kernels, mixer_terms(): pl.pallas_call(functools.partial(mixer_kernel, together=2), name='mixer_t...  33.2 us
    pallas_call x1, Pallas kernels, finish_mix(): pl.pallas_call(finish_kernel, name='finish_mix', out_shape=jax.ShapeDtype...  8.33 us
    dot_general x1, matrix products, body(): jnp.dot(token_major, lax.all_gather(output_weight, TP, axis=0, tiled=True...  5.04 us
  transfers between devices with their start and end apart: 1, of which 0 were waited for; matrix products, arithmetic and copies ran while one was open for 2% of the time, Pallas kernels for 31%

profile of v2, /device:TPU:6, one launch (start us, length us, event | category | flops | bytes accessed | tf_op | source)
XLA Modules:
  0.0 225.6 jit_solution(9411191447986890828)
XLA Ops:
  6.5 0.0 all-gather.2.cloned.1.call-start
  6.5 0.7 all-gather.2.cloned.1.call-update
  7.3 1.6 copy.33.spike_ref
  8.8 33.2 %mixer_terms.1 = (f32[512,128]{1,0:T(8,128)}, f32[512,256]{1,0:T(8,128)}, f32[2,8,64,128]{3,2,1,0:T(8,128)}, f32[2,8,64,128]{3,2,1,0:T(8,128)}, bf16[2,128,128]{2,1,0:T(8,128)(2,1)}) custom-call(bf16[512,128]{1,0:T(8,128)(2,1)} %read_ref.1, bf16[512,128]{1,0:T(8,128)(2,1)} %key_ref.1, bf16[512,128]{1,0:T(8,128)(2,1)} %value_ref.1, ...), custom_call_target="tpu_custom_call" | custom-call | tf_op jit(solution)/shard_map/mixer_terms/pallas_call | solution.py:229
  42.1 14.4 %states.1.got_ref = bf16[16,128,128]{2,1,0:T(8,128)(2,1)} custom-call(bf16[2,128,128]{2,1,0:T(8,128)(2,1)} %get-tuple-element.10.x_ref), custom_call_target="tpu_custom_call" | custom-call | tf_op jit(solution)/shard_map/states/pallas_call | solution.py:314
  56.4 8.3 %finish_mix.1 = bf16[512,128]{1,0:T(8,128)(2,1)} custom-call(s32[1]{0:T(128)} %bitcast.place_ref, bf16[16,128,128]{2,1,0:T(8,128)(2,1)} %states.1.got_ref, f32[512,128]{1,0:T(8,128)} %get-tuple-element.11.local_ref, f32[512,256]{1,0:T(8,128)} %get-tuple-element.12.readout_ref, f32[2,8,64,128]{3,2,1,0:T(8,128)} %get-tuple-element.13.prefix_ref, ...), custom_call_target="tpu_custom_call" | custom-call | tf_op jit(solution)/shard_map/finish_mix/pallas_call | solution.py:281
  64.8 13.7 %heads.1 = bf16[32,2048]{1,0:T(8,128)(2,1)} custom-call(bf16[16,32,128]{2,1,0:T(8,128)(2,1)} %bitcast.19), custom_call_target="tpu_custom_call" | custom-call | tf_op jit(solution)/shard_map/heads/pallas_call | solution.py:314
  78.5 0.7 convert_element_type.47
  79.2 0.8 copy.34
  79.9 0.1 eq.57
  80.0 0.1 fusion.9
  80.1 0.1 reduce_window_sum.11
  80.2 0.2 select_reduce_fusion.1
  80.4 0.1 reduce_sum.39
  80.5 0.1 copy.39
  80.6 0.8 select_reduce_fusion
  81.4 0.0 all-gather.2.cloned.1.call-done
  81.4 5.0 %multiply_reduce_fusion = (f32[32]{0:T(128)S(1)}, f32[32,2048]{1,0:T(8,128)S(1)}) fusion(bf16[32,2048]{1,0:T(8,128)(2,1)} %heads.1, bf16[2048,2048]{1,0:T(8,128)(2,1)} %all-gather.2.cloned.1.call-done, bf16[32,2048]{1,0:T(8,128)(2,1)} %param.18), kind=kOutput, calls=%fused_computation.16 | convolution fusion | flops 268697568 | bytes 8913024 | tf_op jit(solution)/shard_map/dot_general | solution.py:648
  86.5 0.1 multiply_convert_fusion
  86.6 1.1 fusion.x_ref
  87.7 14.7 %to_experts.1 = bf16[16,8,2048]{2,1,0:T(8,128)(2,1)} custom-call(bf16[16,8,2048]{2,1,0:T(8,128)(2,1)} %fusion.x_ref), custom_call_target="tpu_custom_call" | custom-call | tf_op jit(solution)/shard_map/to_experts/pallas_call | solution.py:314
  102.4 1.4 convolution_convert_fusion.2
  103.7 0.8 pad_maximum_fusion.x_ref
  104.6 94.1 %experts.1 = bf16[128,2048]{1,0:T(8,128)(2,1)} custom-call(bf16[128,2048]{1,0:T(8,128)(2,1)} %pad_maximum_fusion.x_ref, bf16[2,2048,256]{2,1,0:T(8,128)(2,1)} %expert_gate.1, bf16[2,2048,256]{2,1,0:T(8,128)(2,1)} %expert_up.1, bf16[2,256,2048]{2,1,0:T(8,128)(2,1)} %expert_down.1, bf16[2048,256]{1,0:T(8,128)(2,1)} %shared_gate.1, ...), custom_call_target="tpu_custom_call" | custom-call | tf_op jit(solution)/shard_map/experts/pallas_call | solution.py:579
  198.7 2.2 fusion.1.x_ref
  201.0 14.6 %to_tokens.1 = bf16[16,8,2048]{2,1,0:T(8,128)(2,1)} custom-call(bf16[16,8,2048]{2,1,0:T(8,128)(2,1)} %fusion.1.x_ref), custom_call_target="tpu_custom_call" | custom-call | tf_op jit(solution)/shard_map/to_tokens/pallas_call | solution.py:314
  215.6 1.2 fusion.5
  216.8 1.9 fusion.3
  (3 shorter events, 0.1 us)
Async XLA Ops:
  6.5 74.9 %all-gather.2.cloned.1.call-start = ((), (), s32[]{:S(2)}) async-start(), calls=%async_computation | async-start | bytes 8912896 | tf_op jit(solution)/shard_map/all_gather | solution.py:650
Sparse Core Ops, SparseCore 0:
  9.2 58.9 all-gather.1

commit v3 on v1

v3 whole, which is shorter than its diff:
```python
import functools

import jax
import jax.numpy as jnp
from jax import lax
from jax.experimental import pallas as pl
from jax.experimental.pallas import tpu as pltpu
from jax.sharding import PartitionSpec as P

SP = "sp"
TP = "tp"
BLOCK = 64
LANES = 128
GN_EPS = 0.00064
RMS_EPS = 1e-06
f32 = jnp.float32
bf16 = jnp.bfloat16
VMEM = pl.BlockSpec(memory_space=pltpu.VMEM)
NN = (((1,), (0,)), ((), ()))
NT = (((1,), (1,)), ((), ()))
TN = (((0,), (0,)), ((), ()))


def iota(shape, dim):
    return lax.broadcasted_iota(jnp.int32, shape, dim)


def halves(array):
    high = array.astype(bf16)
    return high, (array - high.astype(f32)).astype(bf16)


def raw_dot(left, right, dims):
    return lax.dot_general(left, right, dims, preferred_element_type=f32)


def head_mask(count, dtype):
    first = (iota((count, LANES), 1) < BLOCK).astype(f32)
    return first.astype(dtype), (1.0 - first).astype(dtype)


def both_heads(rows):
    first, second = head_mask(rows.shape[0], rows.dtype)
    return jnp.concatenate([rows * first, rows * second], axis=0)


def fine_dot(left, right, dims, spread=False):
    left_high, left_low = halves(left)
    right_high, right_low = halves(right)
    if spread:
        right_high, right_low = both_heads(right_high), both_heads(right_low)
    if dims == TN:
        return raw_dot(
            jnp.concatenate([left_high, left_high, left_low], axis=0),
            jnp.concatenate([right_high, right_low, right_high], axis=0),
            TN,
        )
    count = left.shape[0]
    both = raw_dot(jnp.concatenate([left_high, left_low], axis=0), right_high, dims)
    return both[:count] + both[count:] + raw_dot(left_high, right_low, dims)


def exact_right_dot(left, right, dims):
    left_high, left_low = halves(left)
    count = left.shape[0]
    both = raw_dot(jnp.concatenate([left_high, left_low], axis=0), right, dims)
    return both[:count] + both[count:]


def head_sum(rows):
    ones = (iota((LANES, LANES), 0) // BLOCK == iota((LANES, LANES), 1) // BLOCK).astype(bf16)
    return exact_right_dot(rows, ones, NN)


def block_sums(log_decay):
    high = log_decay.astype(bf16)
    rest = log_decay - high.astype(f32)
    middle = rest.astype(bf16)
    low = (rest - middle.astype(f32)).astype(bf16)
    count = log_decay.shape[0]
    ones = (iota((count, count), 0) >= iota((count, count), 1)).astype(bf16)
    width = log_decay.shape[1]
    sums = raw_dot(ones, jnp.concatenate([high, middle, low], axis=1), NN)
    return sums[:, :width] + sums[:, width : 2 * width] + sums[:, 2 * width :]


def inverses(stricts):
    row, lane = iota((BLOCK, LANES), 0), iota((BLOCK, LANES), 1) % BLOCK

    def within(size):
        return row // size == lane // size

    def products(lefts, rights):
        return [fine_dot(left, right, NN, spread=True) for left, right in zip(lefts, rights)]

    smalls = [jnp.where(within(8), strict, 0.0) for strict in stricts]
    starts = [jnp.where(row == lane, 1.0, 0.0) - small for small in smalls]
    squares = products(smalls, smalls)
    boths = products([jnp.concatenate(p, axis=0) for p in zip(starts, squares)], squares)
    results = [start + both[:BLOCK] for start, both in zip(starts, boths)]
    more = products(results, [both[BLOCK:] for both in boths])
    results = [r + m for r, m in zip(results, more)]
    for size in (8, 16, 32):
        keep = within(2 * size) & ~within(size)
        edges = products(results, [jnp.where(keep, strict, 0.0) for strict in stricts])
        more = products(edges, results)
        results = [r - m for r, m in zip(results, more)]
    return results


def block_terms(chains):
    row, lane = iota((BLOCK, LANES), 0), iota((BLOCK, LANES), 1) % BLOCK
    scaled, pairs = [], []
    for unit, beta, key_rows, _, read, left_unit, left_read, right, _, _ in chains:
        scaled.append((unit * left_unit, read * left_read, beta * right, key_rows * right))
    for unit_mid, read_mid, beta_mid, key_mid in scaled:
        left_high, left_low = halves(jnp.concatenate([unit_mid, read_mid], axis=0))
        right_high, right_low = [
            jnp.concatenate([both_heads(b), both_heads(k)], axis=0)
            for b, k in zip(halves(beta_mid), halves(key_mid))
        ]
        both = raw_dot(jnp.concatenate([left_high, left_low], axis=0), right_high, NT)
        pairs.append(both[: 2 * BLOCK] + both[2 * BLOCK :] + raw_dot(left_high, right_low, NT))
    erase_betas, keyeds, read_betas = [], [], []
    for pair, chain in zip(pairs, chains):
        strict = row > lane if chain[-1] else row < lane
        upto = row >= lane if chain[-1] else row <= lane
        erase_betas.append(jnp.where(strict, pair[:BLOCK, :LANES], 0.0))
        erase_key = jnp.where(strict, pair[:BLOCK, LANES:], 0.0)
        read_betas.append(jnp.where(upto, pair[BLOCK:, :LANES], 0.0))
        read_key = jnp.where(upto, pair[BLOCK:, LANES:], 0.0)
        keyeds.append(
            exact_right_dot(jnp.concatenate([erase_key, read_key], axis=0), chain[3], NN)
        )
    solvers = inverses(erase_betas)
    solved = []
    for solver, (unit_mid, _, _, _), keyed, chain in zip(solvers, scaled, keyeds, chains):
        solver_high, solver_low = halves(solver)
        right_high, right_low = [
            jnp.concatenate([both_heads(u), both_heads(k)], axis=1)
            for u, k in zip(halves(unit_mid * chain[8]), halves(-keyed[:BLOCK]))
        ]
        both = raw_dot(jnp.concatenate([solver_high, solver_low], axis=0), right_high, NN)
        solved.append(both[:BLOCK] + both[BLOCK:] + raw_dot(solver_high, right_low, NN))
    terms = []
    for found, read_beta, keyed, scale, chain in zip(solved, read_betas, keyeds, scaled, chains):
        spread_parts = [
            jnp.concatenate([both_heads(p[:, :LANES]), both_heads(p[:, LANES:])], axis=1)
            for p in halves(found)
        ]
        read_high, read_low = halves(read_beta)
        both = raw_dot(jnp.concatenate([read_high, read_low], axis=0), spread_parts[0], NN)
        applied = both[:BLOCK] + both[BLOCK:] + raw_dot(read_high, spread_parts[1], NN)
        readout = scale[1] * chain[8] - applied[:, :LANES]
        local = applied[:, LANES:] + keyed[BLOCK:]
        terms.append((found, scale[2] * chain[8], scale[3] * chain[8], readout, local))
    return terms


def mixer_kernel(
    read_ref,
    key_ref,
    value_ref,
    erase_ref,
    decay_ref,
    spike_ref,
    local_ref,
    readout_ref,
    prefix_ref,
    start_ref,
    got_ref,
    move_ref,
    carry_ref,
    whole_ref,
    send_sem,
    recv_sem,
    *,
    together,
):
    barrier, expected = meet_peers(SP, got_ref.shape[0], [])
    tokens = key_ref.shape[0]
    block_count = tokens // BLOCK
    lane = iota((BLOCK, LANES), 1)
    same_head = iota((LANES, LANES), 0) // BLOCK == iota((LANES, LANES), 1) // BLOCK
    diagonal = iota((LANES, LANES), 0) == iota((LANES, LANES), 1)

    def some_blocks(blocks):
        chains, totals, values = [], [], []
        places = [pl.ds(pl.multiple_of(block * BLOCK, BLOCK), BLOCK) for block in blocks]
        for at in places:
            key_rows = key_ref[at, :].astype(f32)
            read = read_ref[at, :].astype(f32)
            value = value_ref[at, :]
            unit = key_rows * lax.rsqrt(head_sum(key_rows * key_rows) + 1e-06)
            beta = unit * jax.nn.sigmoid(erase_ref[at, :].astype(f32))
            decay_in = decay_ref[at, :].astype(f32)
            spike = jnp.where(lane < BLOCK, spike_ref[at, 0:1], spike_ref[at, 1:2])
            log_decay = -jnp.exp(-jax.nn.softplus(-decay_in) - 0.5) + spike
            upto = block_sums(log_decay)
            total = upto[BLOCK - 1 :, :]
            middle = 0.5 * total
            ahead = upto - log_decay
            before, after = jnp.exp(ahead - middle), jnp.exp(upto - middle)
            until, since = jnp.exp(middle - upto), jnp.exp(middle - ahead)
            edge = jnp.exp(middle)
            shared = (unit, beta, key_rows, both_heads(value), read)
            chains.append(shared + (before, after, until, edge, True))
            chains.append(shared + (until, since, before, edge, False))
            totals.append(total)
            values.append(value)
        terms = block_terms(chains)
        for k, at in enumerate(places):
            local_ref[at, :] = terms[2 * k][4] + terms[2 * k + 1][4]
        for k, (solved, beta_end, key_end, readout, _) in enumerate(terms):
            way, at, value = k % 2, places[k // 2], values[k // 2]
            readout_ref[at, way * LANES : (way + 1) * LANES] = readout
            moved = fine_dot(solved, beta_end, TN)
            key_high, key_low = halves(key_end)
            keyed = raw_dot(
                jnp.concatenate([value, value], axis=0),
                jnp.concatenate([key_high, key_low], axis=0),
                TN,
            )
            move_ref[way, blocks[k // 2]] = jnp.where(
                same_head, jnp.where(diagonal, jnp.exp(totals[k // 2]), 0.0) - moved[:LANES], 0.0
            )
            carry = jnp.where(same_head, moved[LANES:] + keyed, 0.0)
            carry_ref[way, blocks[k // 2]] = carry[:BLOCK] + carry[BLOCK:]

    def step(index, _):
        some_blocks([index * together + k for k in range(together)])
        return 0

    lax.fori_loop(0, block_count // together, step, 0)
    identity = jnp.where(iota((BLOCK, LANES), 0) == iota((BLOCK, LANES), 1) % BLOCK, 1.0, 0.0)
    running = [jnp.concatenate([identity, jnp.zeros_like(identity)], axis=0)] * 2
    for k in range(block_count):
        for way in range(2):
            block = k if way == 0 else block_count - 1 - k
            now = running[way]
            prefix_ref[way, block] = now[:BLOCK]
            start_ref[way, block] = now[BLOCK:]
            after = fine_dot(now, move_ref[way, block], NN)
            running[way] = jnp.concatenate(
                [after[:BLOCK], after[BLOCK:] + carry_ref[way, block]], axis=0
            )
    for way in range(2):
        whole_ref[way] = running[way].astype(bf16)
    pl.semaphore_wait(barrier, expected)
    me, count = lax.axis_index(SP), got_ref.shape[0]
    states = Push(
        SP,
        lambda peer: whole_ref.at[(me + count - peer) // (count + 1)],
        got_ref,
        (send_sem, recv_sem),
    )
    states.begin()
    states.arrive()
    states.leave()


def mixer_terms(read, keys, values, erase, decay, spike, sp_count, number):
    tokens = keys.shape[0]
    block_count = tokens // BLOCK
    shape = jax.ShapeDtypeStruct
    return pl.pallas_call(
        functools.partial(mixer_kernel, together=4),
        name="mixer_terms",
        out_shape=(
            shape((tokens, LANES), f32),
            shape((tokens, 2 * LANES), f32),
            shape((2, block_count, BLOCK, LANES), f32),
            shape((2, block_count, BLOCK, LANES), f32),
            shape((sp_count, 2 * BLOCK, LANES), bf16),
        ),
        in_specs=[VMEM] * 6,
        out_specs=[VMEM] * 5,
        scratch_shapes=[
            pltpu.VMEM((2, block_count, LANES, LANES), f32),
            pltpu.VMEM((2, block_count, BLOCK, LANES), f32),
            pltpu.VMEM((2, 2 * BLOCK, LANES), bf16),
            pltpu.SemaphoreType.DMA((sp_count,)),
            pltpu.SemaphoreType.DMA((sp_count,)),
        ],
        compiler_params=pltpu.CompilerParams(collective_id=number, has_side_effects=True),
    )(read, keys, values, erase, decay, spike)


class Ring:
    def __init__(self, axis, chips):
        self.axis, self.chips = axis, chips
        self.me = lax.axis_index(axis)
        self.chip, self.core = self.me // 2, lax.rem(self.me, 2)
        self.steps = chips - 1
        self.far = chips // 2
        self.next = (self.slot(1, self.core), self.slot(-1, self.core))
        self.twin = self.chip * 2 + 1 - self.core
        self.sent = []

    def chip_at(self, distance):
        return lax.rem(self.chip + distance + self.chips, self.chips)

    def slot(self, distance, which):
        return self.chip_at(distance) * 2 + which

    def copy(self, source, target, send, recv, peer):
        return pltpu.make_async_remote_copy(
            src_ref=source, dst_ref=target, send_sem=send, recv_sem=recv, device_id={self.axis: peer}
        )

    def start(self, copy):
        copy.start()
        self.sent.append(copy)

    def half_of(self, way, step):
        return step % 2 if way == 0 else 1 - step % 2


class Gather:
    def __init__(self, ring, own, blocks, sems):
        self.ring, self.own, self.blocks = ring, own, blocks
        self.send, self.recv, self.pass_send, self.pass_recv = sems
        self.half = own.shape[0] // 2

    def piece(self, way, step):
        return pl.ds(self.ring.half_of(way, step) * self.half, self.half)

    def hop(self, way, step):
        ring, piece = self.ring, self.piece(way, step)
        at = ring.slot((step // 2) * (-1 if way == 0 else 1), ring.core)
        source = self.own.at[piece] if step < 2 else self.blocks.at[at, piece]
        return ring.copy(
            source,
            self.blocks.at[at, piece],
            self.send.at[way, step],
            self.recv.at[way, step],
            ring.next[way],
        )

    def hand(self, way, step):
        ring, piece = self.ring, self.piece(way, step)
        at = ring.slot((step // 2 + 1) * (-1 if way == 0 else 1), ring.core)
        return ring.copy(
            self.blocks.at[at, piece],
            self.blocks.at[at, piece],
            self.pass_send.at[way, step],
            self.pass_recv.at[way, step],
            ring.twin,
        )

    def hand_own(self):
        ring = self.ring
        return ring.copy(
            self.own,
            self.blocks.at[ring.me],
            self.pass_send.at[0, ring.steps],
            self.pass_recv.at[0, ring.steps],
            ring.twin,
        )

    def begin(self):
        for step in (0, 1):
            for way in (0, 1):
                self.ring.start(self.hop(way, step))
        self.ring.start(self.hand_own())
        self.blocks[self.ring.me] = self.own[...]

    def advance(self, step):
        for way in (0, 1):
            self.hop(way, step).wait_recv()
            if step + 2 < self.ring.steps:
                self.ring.start(self.hop(way, step + 2))
            self.ring.start(self.hand(way, step))

    def handed(self, *steps):
        for step in steps:
            for way in (0, 1):
                self.hand(way, step).wait_recv()


class Sum:
    def __init__(self, ring, partial, other, inbox, sems):
        self.ring, self.partial, self.other, self.inbox = ring, partial, other, inbox
        self.pair_send, self.pair_recv, self.send_sem, self.recv_sem = sems
        self.half = partial.shape[1] // 2
        self.met = set()

    def pair(self, distance):
        ring = self.ring
        index = ring.chip_at(distance)
        return ring.copy(
            self.partial.at[ring.slot(distance, 1 - ring.core)],
            self.other.at[index],
            self.pair_send.at[index],
            self.pair_recv.at[index],
            ring.twin,
        )

    def give(self, *distances):
        for distance in distances:
            self.ring.start(self.pair(distance))

    def meet(self, distance):
        key = distance % self.ring.chips
        if key not in self.met:
            self.met.add(key)
            self.pair(distance).wait_recv()

    def place(self, way, step):
        ring = self.ring
        distance = (ring.far - (step + 1) // 2) * (1 if way == 0 else -1)
        return distance, pl.ds(ring.half_of(way, step) * self.half, self.half)

    def hop(self, way, step):
        ring = self.ring
        distance, piece = self.place(way, step)
        return ring.copy(
            self.partial.at[ring.slot(distance, ring.core), piece],
            self.inbox.at[way, step],
            self.send_sem.at[way, step],
            self.recv_sem.at[way, step],
            ring.next[way],
        )

    def both_cores(self, distance, piece):
        ring = self.ring
        return self.partial[ring.slot(distance, ring.core), piece, :].astype(f32) + self.other[
            ring.chip_at(distance), piece, :
        ].astype(f32)

    def advance(self, step):
        ring = self.ring
        for way in (0, 1):
            distance, piece = self.place(way, step)
            self.meet(distance)
            total = self.both_cores(distance, piece)
            if step >= 2:
                self.hop(way, step - 2).wait_recv()
                total = total + self.inbox[way, step - 2].astype(f32)
            self.partial[ring.slot(distance, ring.core), piece, :] = total.astype(bf16)
        for way in (0, 1):
            ring.start(self.hop(way, step))

    def own_half(self, which):
        ring = self.ring
        self.meet(0)
        total = self.both_cores(0, pl.ds(which * self.half, self.half))
        for way in (0, 1):
            step = ring.steps - 2 if ring.half_of(way, ring.steps - 2) == which else ring.steps - 1
            self.hop(way, step).wait_recv()
            total = total + self.inbox[way, step].astype(f32)
        return total


class Push:
    def __init__(self, axis, source, target, sems):
        self.axis, self.source, self.target = axis, source, target
        self.send, self.recv = sems
        self.count = target.shape[0]
        self.me = lax.axis_index(axis)
        self.copies = []

    def begin(self):
        for k in range(1, self.count):
            peer = lax.rem(self.me + k, self.count)
            copy = pltpu.make_async_remote_copy(
                src_ref=self.source(peer),
                dst_ref=self.target.at[self.me],
                send_sem=self.send.at[k],
                recv_sem=self.recv.at[k],
                device_id={self.axis: peer},
            )
            copy.start()
            self.copies.append(copy)
        self.target[self.me] = self.source(self.me)[...]

    def arrive(self):
        for copy in self.copies:
            copy.wait_recv()

    def leave(self):
        for copy in self.copies:
            copy.wait_send()


def meet_peers(axis, count, others):
    me = lax.axis_index(axis)
    barrier = pltpu.get_barrier_semaphore()
    for k in range(1, count):
        pl.semaphore_signal(barrier, inc=1, device_id={axis: lax.rem(me + k, count)})
    for name, peer in others:
        pl.semaphore_signal(barrier, inc=1, device_id={name: peer})
    return barrier, count - 1 + len(others)


def finish_blocks(place, got_ref, local_ref, readout_ref, prefix_ref, start_ref, gain_ref, mixed_ref):
    count = got_ref.shape[0]
    blocks = range(prefix_ref.shape[1])
    entry = [jnp.zeros((BLOCK, LANES), f32)] * 2
    for k in range(count - 1):
        for way in range(2):
            j = k if way == 0 else count - 1 - k
            passed = j < place if way == 0 else j > place
            moved = exact_right_dot(entry[way], both_heads(got_ref[j, :BLOCK, :]), NN)
            entry[way] = jnp.where(passed, moved + got_ref[j, BLOCK:, :].astype(f32), entry[way])
    gain = gain_ref[...].astype(f32)
    states = []
    for way in range(2):
        high, low = halves(entry[way])
        stacked = jnp.concatenate([high, low], axis=0)
        prefixes = [[both_heads(p) for p in halves(prefix_ref[way, b])] for b in blocks]
        boths = [raw_dot(stacked, p[0], NN) for p in prefixes]
        rests = [raw_dot(high, p[1], NN) for p in prefixes]
        states.append(
            [
                [both_heads(p) for p in halves(x[:BLOCK] + x[BLOCK:] + y + start_ref[way, b])]
                for x, y, b in zip(boths, rests, blocks)
            ]
        )
    places = [slice(b * BLOCK, (b + 1) * BLOCK) for b in blocks]
    mixes = []
    for b in blocks:
        state_high, state_low = [
            jnp.concatenate([states[0][b][k], states[1][b][k]], axis=1) for k in (0, 1)
        ]
        read_high, read_low = halves(readout_ref[places[b], :])
        both = raw_dot(jnp.concatenate([read_high, read_low], axis=0), state_high, NT)
        mixes.append(
            local_ref[places[b], :] + both[:BLOCK] + both[BLOCK:] + raw_dot(read_high, state_low, NT)
        )
    centers = [mix - head_sum(mix) * (1.0 / BLOCK) for mix in mixes]
    spreads = [head_sum(center * center) * (1.0 / BLOCK) for center in centers]
    for b in blocks:
        mixed_ref[places[b], :] = (centers[b] * lax.rsqrt(spreads[b] + GN_EPS) * gain).astype(bf16)


def layer_kernel(
    got_ref,
    local_ref,
    readout_ref,
    prefix_ref,
    start_ref,
    gain_ref,
    mix_weight_ref,
    input_ref,
    norm_gain_ref,
    placing_ref,
    weighting_ref,
    packing_ref,
    expert_gate,
    expert_up,
    expert_down,
    shared_gate,
    shared_up,
    shared_down,
    o_ref,
    mixed,
    residual,
    normed,
    outgoing,
    arrived,
    packed,
    unpacked,
    returned,
    shared_blocks,
    routed_blocks,
    mix_partial,
    shared_partial,
    routed_partial,
    mix_other,
    shared_other,
    routed_other,
    mix_inbox,
    shared_inbox,
    routed_inbox,
    gate,
    up,
    down,
    weight_sem,
    *sems,
    devices,
    sp_count,
):
    ring = Ring(TP, devices // 2)
    local_experts = expert_gate.shape[0]
    width = input_ref.shape[1]
    used = packing_ref.shape[0] // local_experts
    weight_copies = []
    for k, (pair, single, into) in enumerate(
        ((expert_gate, shared_gate, gate), (expert_up, shared_up, up), (expert_down, shared_down, down))
    ):
        weight_copies.append(
            pltpu.make_async_copy(pair, into.at[pl.ds(0, local_experts)], weight_sem.at[2 * k])
        )
        weight_copies.append(
            pltpu.make_async_copy(single, into.at[local_experts], weight_sem.at[2 * k + 1])
        )
    for copy in weight_copies:
        copy.start()
    barrier, expected = meet_peers(
        SP, sp_count, [(TP, ring.next[0]), (TP, ring.next[1]), (TP, ring.twin)]
    )

    finish_blocks(
        lax.axis_index(SP), got_ref, local_ref, readout_ref, prefix_ref, start_ref, gain_ref, mixed
    )
    columns = 512

    def project(k, _):
        at = pl.ds(pl.multiple_of(k * columns, columns), columns)
        product = raw_dot(mixed[...], mix_weight_ref[:, at], NN).astype(bf16)
        mix_partial[:, :, at] = product.reshape(mix_partial.shape[0], mix_partial.shape[1], columns)
        return 0

    lax.fori_loop(0, width // columns, project, 0)
    pl.semaphore_wait(barrier, expected)
    mix_sum = Sum(ring, mix_partial, mix_other, mix_inbox, sems[0:4])
    mix_sum.give(ring.far, ring.far - 1, 1 - ring.far, *range(ring.far - 2, 1 - ring.far, -1))
    for step in range(ring.steps):
        mix_sum.advance(step)
    half = residual.shape[0] // 2
    for which in (0, 1):
        piece = slice(which * half, (which + 1) * half)
        rows = input_ref[piece, :].astype(f32) + mix_sum.own_half(which)
        residual[piece, :] = rows
        scale = lax.rsqrt(jnp.mean(rows * rows, axis=-1, keepdims=True) + RMS_EPS)
        normed[piece, :] = (rows * scale * norm_gain_ref[...].astype(f32)).astype(bf16)

    shared_in = Gather(ring, normed, shared_blocks, sems[4:8])
    outgoing[...] = (
        raw_dot(placing_ref[...], normed[...], TN).astype(bf16).reshape(outgoing.shape)
    )
    shared_in.begin()
    dispatch = Push(SP, lambda peer: outgoing.at[peer], arrived, sems[8:10])
    dispatch.begin()
    for step in range(ring.steps - 1):
        shared_in.advance(step)
    dispatch.arrive()
    packed[...] = raw_dot(
        packing_ref[...], arrived[...].reshape(packing_ref.shape[1], width), NN
    ).astype(bf16)
    routed_in = Gather(ring, packed, routed_blocks, sems[10:14])
    routed_in.begin()
    shared_in.advance(ring.steps - 1)

    def expert_on(blocks, partial, first, count, at, which):
        rows = at.size
        x = blocks[pl.ds(first, count), at, :].reshape(count * rows, width)
        gated = raw_dot(x, gate[which], NN)
        lifted = raw_dot(x, up[which], NN)
        inner = (gated / (1.0 + jnp.exp(-gated)) * lifted).astype(bf16)
        partial[pl.ds(first, count), at, :] = (
            raw_dot(inner, down[which], NN).astype(bf16).reshape(count, rows, width)
        )

    def routed_on(distance):
        first = ring.chip_at(distance) * 2

        def one(k, _):
            at = pl.ds(pl.multiple_of(k * used, 16), used)
            expert_on(routed_blocks, routed_partial, first, 2, at, k)
            return 0

        lax.fori_loop(0, local_experts, one, 0)

    def shared_on(quarter):
        count = devices // 4
        at = pl.ds(0, normed.shape[0])
        expert_on(shared_blocks, shared_partial, quarter * count, count, at, local_experts)

    routed_sum = Sum(ring, routed_partial, routed_other, routed_inbox, sems[14:18])
    shared_sum = Sum(ring, shared_partial, shared_other, shared_inbox, sems[18:22])
    for copy in weight_copies:
        copy.wait()
    shared_in.hand_own().wait_recv()
    shared_in.handed(*range(ring.steps))

    def quarters(first):
        def one(k, _):
            shared_on(first + k)
            return 0

        lax.fori_loop(0, 2, one, 0)

    quarters(0)
    for step in range(ring.steps):
        routed_in.advance(step)
        if step == 0:
            quarters(2)
        elif step % 2 == 1:
            distance = (step + 1) // 2
            routed_in.handed(step - 1, step)

            def both(k, _):
                routed_on(distance * (2 * k - 1))
                return 0

            lax.fori_loop(0, 2, both, 0)
        elif step == 2:
            routed_in.hand_own().wait_recv()
            routed_on(0)
            routed_sum.give(-1, 1)
        elif step == 4:
            routed_sum.give(0, -2, 2)
        elif step == 6:
            routed_sum.give(-3, 3)
    routed_in.handed(ring.steps - 1)
    routed_on(ring.far)
    routed_sum.give(ring.far)
    shared_sum.give(ring.far, ring.far - 1, 1 - ring.far, *range(ring.far - 2, 1 - ring.far, -1))
    for step in range(ring.steps):
        routed_sum.advance(step)
    shared_sum.advance(0)
    shared_sum.advance(1)
    summed = jnp.concatenate([routed_sum.own_half(which).astype(bf16) for which in (0, 1)], axis=0)
    unpacked[...] = raw_dot(packing_ref[...], summed, TN).astype(bf16).reshape(unpacked.shape)
    back = Push(SP, lambda peer: unpacked.at[peer], returned, sems[22:24])
    back.begin()
    for step in range(2, ring.steps):
        shared_sum.advance(step)
    half = residual.shape[0] // 2
    for which in (0, 1):
        piece = slice(which * half, (which + 1) * half)
        residual[piece, :] = residual[piece, :] + shared_sum.own_half(which)
    back.arrive()
    rows = returned[...].reshape(weighting_ref.shape[1], width)
    routed = exact_right_dot(weighting_ref[...], rows, NN)
    o_ref[...] = (residual[...] + routed).astype(bf16)
    for copy in ring.sent:
        copy.wait_send()
    dispatch.leave()
    back.leave()


def layer(arrays, weights, devices, sp_count, room, number, name):
    got, local, readout, prefix, start, gain, mix_weight, layer_input, norm_gain = arrays[:9]
    placing, weighting, packing = arrays[9:]
    rows, width = layer_input.shape
    hidden = weights[3].shape[1]
    local_experts = weights[0].shape[0]
    packed_rows = packing.shape[0]
    chips = devices // 2
    steps = chips - 1
    dma = pltpu.SemaphoreType.DMA
    anywhere = pl.BlockSpec(memory_space=pl.ANY)
    buffer = lambda *shape: pltpu.VMEM(shape, bf16)
    gather_sems = [dma((2, steps)), dma((2, steps)), dma((2, steps + 1)), dma((2, steps + 1))]
    sum_sems = [dma((chips,)), dma((chips,)), dma((2, steps)), dma((2, steps))]
    push_sems = [dma((sp_count,)), dma((sp_count,))]
    return pl.pallas_call(
        functools.partial(layer_kernel, devices=devices, sp_count=sp_count),
        name=name,
        out_shape=jax.ShapeDtypeStruct((rows, width), bf16),
        in_specs=[VMEM] * 12 + [anywhere] * 6,
        out_specs=VMEM,
        scratch_shapes=[
            buffer(*local.shape),
            pltpu.VMEM((rows, width), f32),
            buffer(rows, width),
            buffer(sp_count, room, width),
            buffer(sp_count, room, width),
            buffer(packed_rows, width),
            buffer(sp_count, room, width),
            buffer(sp_count, room, width),
            buffer(devices, rows, width),
            buffer(devices, packed_rows, width),
            buffer(devices, rows, width),
            buffer(devices, rows, width),
            buffer(devices, packed_rows, width),
            buffer(chips, rows, width),
            buffer(chips, rows, width),
            buffer(chips, packed_rows, width),
            buffer(2, steps, rows // 2, width),
            buffer(2, steps, rows // 2, width),
            buffer(2, steps, packed_rows // 2, width),
            buffer(local_experts + 1, width, hidden),
            buffer(local_experts + 1, width, hidden),
            buffer(local_experts + 1, hidden, width),
            dma((6,)),
        ]
        + sum_sems
        + gather_sems
        + push_sems
        + gather_sems
        + sum_sems
        + sum_sems
        + push_sems,
        compiler_params=pltpu.CompilerParams(
            collective_id=number, has_side_effects=True, vmem_limit_bytes=62 * 1024 * 1024
        ),
    )(*arrays, *weights)


def body(
    layer_input,
    receptance,
    keys,
    values,
    erase_preact,
    decay_preact,
    decay_spike,
    head_norm_gain,
    output_weight,
    expert_norm_gain,
    routes,
    routing_weight,
    expert_gate_weight,
    expert_up_weight,
    expert_down_weight,
    shared_gate_weight,
    shared_up_weight,
    shared_down_weight,
):
    sp_count, tp_count = lax.axis_size(SP), lax.axis_size(TP)
    local, readout, prefix, start, got = mixer_terms(
        receptance, keys, values, erase_preact, decay_preact, decay_spike, sp_count, 0
    )
    row_count = layer_input.shape[0]
    top_count = routes.shape[1]
    expert_local = expert_gate_weight.shape[0]
    capacity = 3
    room = 8
    slot_total = sp_count * room
    entries = routes.reshape(-1)
    entry_count = entries.shape[0]
    expert_hot = (entries[:, None] == jnp.arange(expert_local * sp_count)[None, :]).astype(jnp.int32)
    rank_in = jnp.sum((jnp.cumsum(expert_hot, axis=0) - 1) * expert_hot, axis=1)
    slot_of = entries // expert_local * room + entries % expert_local * capacity + rank_in
    slot_hot = slot_of[:, None] == jnp.arange(slot_total)[None, :]
    placing = jnp.sum(
        slot_hot.reshape(row_count, top_count, slot_total).astype(f32), axis=1
    ).astype(bf16)
    weighting = jnp.sum(
        jnp.where(slot_hot, routing_weight.reshape(-1, 1), 0.0).reshape(
            row_count, top_count, slot_total
        ),
        axis=1,
    )
    used = sp_count * capacity
    packed_row = jnp.arange(expert_local * used)
    from_slot = (
        packed_row % used // capacity * room
        + packed_row // used * capacity
        + packed_row % capacity
    )
    packing = (from_slot[:, None] == jnp.arange(slot_total)[None, :]).astype(bf16)
    return layer(
        (
            got,
            local,
            readout,
            prefix,
            start,
            head_norm_gain.reshape(1, -1),
            output_weight,
            layer_input,
            expert_norm_gain.reshape(1, -1),
            placing,
            weighting,
            packing,
        ),
        (
            expert_gate_weight,
            expert_up_weight,
            expert_down_weight,
            shared_gate_weight,
            shared_up_weight,
            shared_down_weight,
        ),
        tp_count,
        sp_count,
        room,
        1,
        "layer",
    )


def solution(mesh):
    both = (SP, TP)
    in_specs = (
        P(both, None),
        P(SP, TP),
        P(SP, TP),
        P(SP, TP),
        P(SP, TP),
        P(SP, TP),
        P(SP, TP),
        P(TP),
        P(TP, None),
        P(),
        P(both, None),
        P(both, None),
        P(SP, None, TP),
        P(SP, None, TP),
        P(SP, TP, None),
        P(None, TP),
        P(None, TP),
        P(TP, None),
    )
    return jax.shard_map(
        body, mesh=mesh, in_specs=in_specs, out_specs=P(both, None), check_vma=False
    )
```

time: 270 us -> 155 us (0.57)
  waiting for transfers between devices: 125 us -> 0 us
  Pallas kernels: 112 us -> 147 us
  between operations: 13.2 us -> 0.04 us
  matrix products: 12.9 us -> 0 us
  local copies, waits for them, and re-layouts: 2.6 us -> 5.44 us
    reduce_scatter x1 -> x0, waiting for transfers between devices: 69.3 us -> none  [body(): lax.psum_scatter(outs.reshape(tp_count * block_rows, model_width), TP, sc...]
    all_gather x2 -> x0, waiting for transfers between devices: 55.4 us -> none  [the longest x1 55.3 us: body(): slab = lax.all_gather(own_block, TP, axis=0, tiled=True)]
    pallas_call x8 -> x2, Pallas kernels: 112 us -> 147 us  [the longest x1 126 us: layer(): pl.pallas_call(functools.partial(layer_kernel, devices=devices, sp_count=...]
    dot_general x6 -> x0, matrix products: 12.9 us -> none  [the longest x1 5.04 us: body(): jnp.dot(token_major, lax.all_gather(output_weight, TP, axis=0, tiled=True...]
  transfers between devices with their start and end apart: 3 -> 0, of which waited for: 2 -> 0; matrix products, arithmetic and copies ran while one was open for 2% -> 0% of each run, Pallas kernels for 26% -> 0%
where the time goes in v3:
time: 155 us
  Pallas kernels  147 us (95%)
  local copies, waits for them, and re-layouts  5.44 us (4%)
  other arithmetic  2.46 us (2%)
    pallas_call x1, Pallas kernels, layer(): pl.pallas_call(functools.partial(layer_kernel, devices=devices, sp_count=...  126 us
    pallas_call x1, Pallas kernels, mixer_terms(): pl.pallas_call(functools.partial(mixer_kernel, together=4), name='mixer_t...  20.8 us
    unnamed x3, local copies, waits for them, and re-layouts  3.87 us

profile of v3, /device:TPU:6, one launch (start us, length us, event | category | flops | bytes accessed | tf_op | source)
XLA Modules:
  0.0 155.0 jit_solution(1235478817018125633)
XLA Ops:
  0.0 1.5 copy.33.spike_ref
  1.5 20.8 %mixer_terms.1 = (f32[512,128]{1,0:T(8,128)}, f32[512,256]{1,0:T(8,128)}, f32[2,8,64,128]{3,2,1,0:T(8,128)}, f32[2,8,64,128]{3,2,1,0:T(8,128)}, bf16[16,128,128]{2,1,0:T(8,128)(2,1)}) custom-call(bf16[512,128]{1,0:T(8,128)(2,1)} %read_ref.1, bf16[512,128]{1,0:T(8,128)(2,1)} %key_ref.1, bf16[512,128]{1,0:T(8,128)(2,1)} %value_ref.1, ...), custom_call_target="tpu_custom_call" | custom-call | tf_op jit(solution)/shard_map/mixer_terms/pallas_call | solution.py:266
  22.3 1.3 reshape.118.norm_gain_ref
  23.6 0.8 copy.34
  24.4 0.1 eq.48
  24.5 0.1 fusion.1
  24.6 0.1 reduce_window_sum.11
  24.7 0.2 select_reduce_fusion.1
  24.8 0.1 reduce_sum.30
  25.0 0.1 copy.39
  25.1 1.4 select_reduce_fusion
  26.5 0.7 fusion.packing_ref
  27.1 126.3 %layer.1 = bf16[32,2048]{1,0:T(8,128)(2,1)} custom-call(bf16[16,128,128]{2,1,0:T(8,128)(2,1)} %get-tuple-element.10.got_ref, f32[512,128]{1,0:T(8,128)} %get-tuple-element.11.local_ref, f32[512,256]{1,0:T(8,128)} %get-tuple-element.12.readout_ref, f32[2,8,64,128]{3,2,1,0:T(8,128)} %get-tuple-element.13.prefix_ref, ...), custom_call_target="tpu_custom_call" | custom-call | tf_op jit(solution)/shard_map/layer/pallas_call | solution.py:750
  153.5 1.6 %copy.41 = bf16[32,2048]{1,0:T(8,128)(2,1)} copy(bf16[32,2048]{1,0:T(8,128)(2,1)} %layer.1) | data formatting | bytes 262144
  (2 shorter events, 0.0 us)

commit v4 on v3

--- a/solution.py
+++ b/solution.py
@@ -73,10 +73,7 @@
 
 
 def block_sums(log_decay):
-    high = log_decay.astype(bf16)
-    rest = log_decay - high.astype(f32)
-    middle = rest.astype(bf16)
-    low = (rest - middle.astype(f32)).astype(bf16)
+    high, middle, low = three_parts(log_decay)
     count = log_decay.shape[0]
     ones = (iota((count, count), 0) >= iota((count, count), 1)).astype(bf16)
     width = log_decay.shape[1]
@@ -157,7 +154,22 @@
     return terms
 
 
-def mixer_kernel(
+def three_parts(array):
+    high = array.astype(bf16)
+    rest = array - high.astype(f32)
+    middle = rest.astype(bf16)
+    return high, middle, (rest - middle.astype(f32)).astype(bf16)
+
+
+def to_columns(rows, pick):
+    chosen = [(pick == k).astype(bf16) for k in range(2)]
+    parts = three_parts(rows)
+    return raw_dot(
+        jnp.concatenate(parts, axis=0), jnp.concatenate([jnp.concatenate(chosen, axis=0)] * 3, axis=0), TN
+    )
+
+
+def mixer_stage(
     read_ref,
     key_ref,
     value_ref,
@@ -168,33 +180,33 @@
     readout_ref,
     prefix_ref,
     start_ref,
-    got_ref,
     move_ref,
     carry_ref,
     whole_ref,
-    send_sem,
-    recv_sem,
-    *,
     together,
 ):
-    barrier, expected = meet_peers(SP, got_ref.shape[0], [])
     tokens = key_ref.shape[0]
     block_count = tokens // BLOCK
-    lane = iota((BLOCK, LANES), 1)
     same_head = iota((LANES, LANES), 0) // BLOCK == iota((LANES, LANES), 1) // BLOCK
     diagonal = iota((LANES, LANES), 0) == iota((LANES, LANES), 1)
 
-    def some_blocks(blocks):
+    def some_blocks(index):
+        blocks = [index * together + k for k in range(together)]
+        span = together * BLOCK
+        spikes = to_columns(
+            spike_ref[:, pl.ds(pl.multiple_of(index * span, span), span)],
+            iota((1, LANES), 1) // BLOCK,
+        )
         chains, totals, values = [], [], []
         places = [pl.ds(pl.multiple_of(block * BLOCK, BLOCK), BLOCK) for block in blocks]
-        for at in places:
+        for k, at in enumerate(places):
             key_rows = key_ref[at, :].astype(f32)
             read = read_ref[at, :].astype(f32)
             value = value_ref[at, :]
             unit = key_rows * lax.rsqrt(head_sum(key_rows * key_rows) + 1e-06)
             beta = unit * jax.nn.sigmoid(erase_ref[at, :].astype(f32))
             decay_in = decay_ref[at, :].astype(f32)
-            spike = jnp.where(lane < BLOCK, spike_ref[at, 0:1], spike_ref[at, 1:2])
+            spike = spikes[k * BLOCK : (k + 1) * BLOCK]
             log_decay = -jnp.exp(-jax.nn.softplus(-decay_in) - 0.5) + spike
             upto = block_sums(log_decay)
             total = upto[BLOCK - 1 :, :]
@@ -228,7 +240,7 @@
             carry_ref[way, blocks[k // 2]] = carry[:BLOCK] + carry[BLOCK:]
 
     def step(index, _):
-        some_blocks([index * together + k for k in range(together)])
+        some_blocks(index)
         return 0
 
     lax.fori_loop(0, block_count // together, step, 0)
@@ -246,44 +258,6 @@
             )
     for way in range(2):
         whole_ref[way] = running[way].astype(bf16)
-    pl.semaphore_wait(barrier, expected)
-    me, count = lax.axis_index(SP), got_ref.shape[0]
-    states = Push(
-        SP,
-        lambda peer: whole_ref.at[(me + count - peer) // (count + 1)],
-        got_ref,
-        (send_sem, recv_sem),
-    )
-    states.begin()
-    states.arrive()
-    states.leave()
-
-
-def mixer_terms(read, keys, values, erase, decay, spike, sp_count, number):
-    tokens = keys.shape[0]
-    block_count = tokens // BLOCK
-    shape = jax.ShapeDtypeStruct
-    return pl.pallas_call(
-        functools.partial(mixer_kernel, together=4),
-        name="mixer_terms",
-        out_shape=(
-            shape((tokens, LANES), f32),
-            shape((tokens, 2 * LANES), f32),
-            shape((2, block_count, BLOCK, LANES), f32),
-            shape((2, block_count, BLOCK, LANES), f32),
-            shape((sp_count, 2 * BLOCK, LANES), bf16),
-        ),
-        in_specs=[VMEM] * 6,
-        out_specs=[VMEM] * 5,
-        scratch_shapes=[
-            pltpu.VMEM((2, block_count, LANES, LANES), f32),
-            pltpu.VMEM((2, block_count, BLOCK, LANES), f32),
-            pltpu.VMEM((2, 2 * BLOCK, LANES), bf16),
-            pltpu.SemaphoreType.DMA((sp_count,)),
-            pltpu.SemaphoreType.DMA((sp_count,)),
-        ],
-        compiler_params=pltpu.CompilerParams(collective_id=number, has_side_effects=True),
-    )(read, keys, values, erase, decay, spike)
 
 
 class Ring:
@@ -534,19 +508,52 @@
         mixed_ref[places[b], :] = (centers[b] * lax.rsqrt(spreads[b] + GN_EPS) * gain).astype(bf16)
 
 
+def routing(routes_ref, weights_ref, room, capacity):
+    rows = routes_ref.shape[1]
+    slot = iota((rows, LANES), 1)
+    within = slot % room
+    second = (within >= capacity).astype(jnp.int32)
+    rank = within - second * capacity
+    in_use = within < 2 * capacity
+    expert = (slot // room * 2 + second).astype(f32)
+    named = []
+    for k in range(2):
+        pick = jnp.full((1, LANES), k, jnp.int32)
+        named.append(
+            (
+                jnp.where((to_columns(routes_ref[...].astype(f32), pick) == expert) & in_use, 1.0, 0.0),
+                to_columns(weights_ref[...], pick),
+            )
+        )
+    either = named[0][0] + named[1][0]
+    before = (iota((rows, rows), 0) > iota((rows, rows), 1)).astype(bf16)
+    taken = raw_dot(before, either.astype(bf16), NN)
+    here = jnp.where(taken == rank.astype(f32), 1.0, 0.0)
+    placing = (either * here).astype(bf16)
+    weighting = (named[0][0] * named[0][1] + named[1][0] * named[1][1]) * here
+    per_expert = LANES // room * capacity
+    shape = (2 * per_expert, LANES)
+    slot = iota(shape, 1)
+    within = slot % room
+    second = (within >= capacity).astype(jnp.int32)
+    target = second * per_expert + slot // room * capacity + within - second * capacity
+    packing = jnp.where((iota(shape, 0) == target) & (within < 2 * capacity), 1.0, 0.0).astype(bf16)
+    return placing, weighting, packing
+
+
 def layer_kernel(
-    got_ref,
-    local_ref,
-    readout_ref,
-    prefix_ref,
-    start_ref,
+    read_ref,
+    key_ref,
+    value_ref,
+    erase_ref,
+    decay_ref,
+    spike_ref,
     gain_ref,
     mix_weight_ref,
     input_ref,
     norm_gain_ref,
-    placing_ref,
-    weighting_ref,
-    packing_ref,
+    routes_ref,
+    route_weights_ref,
     expert_gate,
     expert_up,
     expert_down,
@@ -554,6 +561,14 @@
     shared_up,
     shared_down,
     o_ref,
+    local_ref,
+    readout_ref,
+    prefix_ref,
+    start_ref,
+    move_ref,
+    carry_ref,
+    whole_ref,
+    got_ref,
     mixed,
     residual,
     normed,
@@ -584,7 +599,8 @@
     ring = Ring(TP, devices // 2)
     local_experts = expert_gate.shape[0]
     width = input_ref.shape[1]
-    used = packing_ref.shape[0] // local_experts
+    capacity, room = 3, outgoing.shape[1]
+    used = packed.shape[0] // local_experts
     weight_copies = []
     for k, (pair, single, into) in enumerate(
         ((expert_gate, shared_gate, gate), (expert_up, shared_up, up), (expert_down, shared_down, down))
@@ -601,6 +617,34 @@
         SP, sp_count, [(TP, ring.next[0]), (TP, ring.next[1]), (TP, ring.twin)]
     )
 
+    placing, weighting, packing = routing(routes_ref, route_weights_ref, room, capacity)
+    mixer_stage(
+        read_ref,
+        key_ref,
+        value_ref,
+        erase_ref,
+        decay_ref,
+        spike_ref,
+        local_ref,
+        readout_ref,
+        prefix_ref,
+        start_ref,
+        move_ref,
+        carry_ref,
+        whole_ref,
+        4,
+    )
+    pl.semaphore_wait(barrier, expected)
+    here = lax.axis_index(SP)
+    states = Push(
+        SP,
+        lambda peer: whole_ref.at[(here + sp_count - peer) // (sp_count + 1)],
+        got_ref,
+        sems[24:26],
+    )
+    states.begin()
+    states.arrive()
+
     finish_blocks(
         lax.axis_index(SP), got_ref, local_ref, readout_ref, prefix_ref, start_ref, gain_ref, mixed
     )
@@ -613,22 +657,23 @@
         return 0
 
     lax.fori_loop(0, width // columns, project, 0)
-    pl.semaphore_wait(barrier, expected)
     mix_sum = Sum(ring, mix_partial, mix_other, mix_inbox, sems[0:4])
     mix_sum.give(ring.far, ring.far - 1, 1 - ring.far, *range(ring.far - 2, 1 - ring.far, -1))
     for step in range(ring.steps):
         mix_sum.advance(step)
+    gains = norm_gain_ref[...].astype(f32)
+    norm_gain = jnp.concatenate([gains[k : k + 1] for k in range(gains.shape[0])], axis=1)
     half = residual.shape[0] // 2
     for which in (0, 1):
         piece = slice(which * half, (which + 1) * half)
         rows = input_ref[piece, :].astype(f32) + mix_sum.own_half(which)
         residual[piece, :] = rows
         scale = lax.rsqrt(jnp.mean(rows * rows, axis=-1, keepdims=True) + RMS_EPS)
-        normed[piece, :] = (rows * scale * norm_gain_ref[...].astype(f32)).astype(bf16)
+        normed[piece, :] = (rows * scale * norm_gain).astype(bf16)
 
     shared_in = Gather(ring, normed, shared_blocks, sems[4:8])
     outgoing[...] = (
-        raw_dot(placing_ref[...], normed[...], TN).astype(bf16).reshape(outgoing.shape)
+        raw_dot(placing, normed[...], TN).astype(bf16).reshape(outgoing.shape)
     )
     shared_in.begin()
     dispatch = Push(SP, lambda peer: outgoing.at[peer], arrived, sems[8:10])
@@ -637,7 +682,7 @@
         shared_in.advance(step)
     dispatch.arrive()
     packed[...] = raw_dot(
-        packing_ref[...], arrived[...].reshape(packing_ref.shape[1], width), NN
+        packing, arrived[...].reshape(packing.shape[1], width), NN
     ).astype(bf16)
     routed_in = Gather(ring, packed, routed_blocks, sems[10:14])
     routed_in.begin()
@@ -713,7 +758,7 @@
     shared_sum.advance(0)
     shared_sum.advance(1)
     summed = jnp.concatenate([routed_sum.own_half(which).astype(bf16) for which in (0, 1)], axis=0)
-    unpacked[...] = raw_dot(packing_ref[...], summed, TN).astype(bf16).reshape(unpacked.shape)
+    unpacked[...] = raw_dot(packing, summed, TN).astype(bf16).reshape(unpacked.shape)
     back = Push(SP, lambda peer: unpacked.at[peer], returned, sems[22:24])
     back.begin()
     for step in range(2, ring.steps):
@@ -723,22 +768,23 @@
         piece = slice(which * half, (which + 1) * half)
         residual[piece, :] = residual[piece, :] + shared_sum.own_half(which)
     back.arrive()
-    rows = returned[...].reshape(weighting_ref.shape[1], width)
-    routed = exact_right_dot(weighting_ref[...], rows, NN)
+    rows = returned[...].reshape(weighting.shape[1], width)
+    routed = exact_right_dot(weighting, rows, NN)
     o_ref[...] = (residual[...] + routed).astype(bf16)
     for copy in ring.sent:
         copy.wait_send()
     dispatch.leave()
     back.leave()
-
-
-def layer(arrays, weights, devices, sp_count, room, number, name):
-    got, local, readout, prefix, start, gain, mix_weight, layer_input, norm_gain = arrays[:9]
-    placing, weighting, packing = arrays[9:]
-    rows, width = layer_input.shape
+    states.leave()
+
+
+def layer(arrays, weights, devices, sp_count, capacity, room, number, name):
+    tokens = arrays[1].shape[0]
+    rows, width = arrays[8].shape
     hidden = weights[3].shape[1]
     local_experts = weights[0].shape[0]
-    packed_rows = packing.shape[0]
+    packed_rows = sp_count * local_experts * capacity
+    block_count = tokens // BLOCK
     chips = devices // 2
     steps = chips - 1
     dma = pltpu.SemaphoreType.DMA
@@ -754,7 +800,15 @@
         in_specs=[VMEM] * 12 + [anywhere] * 6,
         out_specs=VMEM,
         scratch_shapes=[
-            buffer(*local.shape),
+            pltpu.VMEM((tokens, LANES), f32),
+            pltpu.VMEM((tokens, 2 * LANES), f32),
+            pltpu.VMEM((2, block_count, BLOCK, LANES), f32),
+            pltpu.VMEM((2, block_count, BLOCK, LANES), f32),
+            pltpu.VMEM((2, block_count, LANES, LANES), f32),
+            pltpu.VMEM((2, block_count, BLOCK, LANES), f32),
+            buffer(2, 2 * BLOCK, LANES),
+            buffer(sp_count, 2 * BLOCK, LANES),
+            buffer(tokens, LANES),
             pltpu.VMEM((rows, width), f32),
             buffer(rows, width),
             buffer(sp_count, room, width),
@@ -784,6 +838,7 @@
         + gather_sems
         + sum_sems
         + sum_sems
+        + push_sems
         + push_sems,
         compiler_params=pltpu.CompilerParams(
             collective_id=number, has_side_effects=True, vmem_limit_bytes=62 * 1024 * 1024
@@ -812,52 +867,20 @@
     shared_down_weight,
 ):
     sp_count, tp_count = lax.axis_size(SP), lax.axis_size(TP)
-    local, readout, prefix, start, got = mixer_terms(
-        receptance, keys, values, erase_preact, decay_preact, decay_spike, sp_count, 0
-    )
-    row_count = layer_input.shape[0]
-    top_count = routes.shape[1]
-    expert_local = expert_gate_weight.shape[0]
-    capacity = 3
-    room = 8
-    slot_total = sp_count * room
-    entries = routes.reshape(-1)
-    entry_count = entries.shape[0]
-    expert_hot = (entries[:, None] == jnp.arange(expert_local * sp_count)[None, :]).astype(jnp.int32)
-    rank_in = jnp.sum((jnp.cumsum(expert_hot, axis=0) - 1) * expert_hot, axis=1)
-    slot_of = entries // expert_local * room + entries % expert_local * capacity + rank_in
-    slot_hot = slot_of[:, None] == jnp.arange(slot_total)[None, :]
-    placing = jnp.sum(
-        slot_hot.reshape(row_count, top_count, slot_total).astype(f32), axis=1
-    ).astype(bf16)
-    weighting = jnp.sum(
-        jnp.where(slot_hot, routing_weight.reshape(-1, 1), 0.0).reshape(
-            row_count, top_count, slot_total
-        ),
-        axis=1,
-    )
-    used = sp_count * capacity
-    packed_row = jnp.arange(expert_local * used)
-    from_slot = (
-        packed_row % used // capacity * room
-        + packed_row // used * capacity
-        + packed_row % capacity
-    )
-    packing = (from_slot[:, None] == jnp.arange(slot_total)[None, :]).astype(bf16)
     return layer(
         (
-            got,
-            local,
-            readout,
-            prefix,
-            start,
+            receptance,
+            keys,
+            values,
+            erase_preact,
+            decay_preact,
+            decay_spike.T,
             head_norm_gain.reshape(1, -1),
             output_weight,
             layer_input,
-            expert_norm_gain.reshape(1, -1),
-            placing,
-            weighting,
-            packing,
+            expert_norm_gain.reshape(-1, LANES),
+            routes.T,
+            routing_weight.T,
         ),
         (
             expert_gate_weight,
@@ -869,8 +892,9 @@
         ),
         tp_count,
         sp_count,
-        room,
-        1,
+        3,
+        8,
+        0,
         "layer",
     )
 

time: 155 us -> 146 us (0.942)
  local copies, waits for them, and re-layouts: 5.44 us -> 1.57 us
  Pallas kernels: 147 us -> 144 us
  other arithmetic: 2.46 us -> 0 us
    pallas_call x1 -> x0, Pallas kernels: 20.8 us -> none  [mixer_terms(): pl.pallas_call(functools.partial(mixer_kernel, together=4), name='mixer_t...]
    pallas_call x1, Pallas kernels: 126 us -> 144 us  [layer(): pl.pallas_call(functools.partial(layer_kernel, devices=devices, sp_count=...]
    unnamed x3 -> x1, local copies, waits for them, and re-layouts: 3.87 us -> 1.57 us
where the time goes in v4:
time: 146 us
  Pallas kernels  144 us (99%)
  local copies, waits for them, and re-layouts  1.57 us (1%)
    pallas_call x1, Pallas kernels, layer(): pl.pallas_call(functools.partial(layer_kernel, devices=devices, sp_count=...  144 us

profile of v4, /device:TPU:6, one launch (start us, length us, event | category | flops | bytes accessed | tf_op | source)
XLA Modules:
  0.0 146.0 jit_solution(12285363573196699213)
XLA Ops:
  0.0 144.4 %layer.1 = bf16[32,2048]{1,0:T(8,128)(2,1)} custom-call(bf16[512,128]{1,0:T(8,128)(2,1)} %read_ref.1, bf16[512,128]{1,0:T(8,128)(2,1)} %key_ref.1, bf16[512,128]{1,0:T(8,128)(2,1)} %value_ref.1, bf16[512,128]{1,0:T(8,128)(2,1)} %erase_ref.1, bf16[512,128]{1,0:T(8,128)(2,1)} %decay_ref.1, f32[2,512]{1,0:T(2,128)} %bitcast.5, bf16[1,128]{1,0:T(2,128)(2,1)} %bitcast.9, ...), custom_call_target="tpu_custom_call" | custom-call | tf_op jit(solution)/shard_map/layer/pallas_call | solution.py:796
  144.4 1.6 %copy.20 = bf16[32,2048]{1,0:T(8,128)(2,1)} copy(bf16[32,2048]{1,0:T(8,128)(2,1)} %layer.1) | data formatting | bytes 262144

commit v5 on v4

--- a/solution.py
+++ b/solution.py
@@ -427,10 +427,10 @@
 
 
 class Push:
-    def __init__(self, axis, source, target, sems):
+    def __init__(self, axis, count, source, target, sems, base=0):
         self.axis, self.source, self.target = axis, source, target
         self.send, self.recv = sems
-        self.count = target.shape[0]
+        self.count, self.base = count, base
         self.me = lax.axis_index(axis)
         self.copies = []
 
@@ -439,14 +439,14 @@
             peer = lax.rem(self.me + k, self.count)
             copy = pltpu.make_async_remote_copy(
                 src_ref=self.source(peer),
-                dst_ref=self.target.at[self.me],
+                dst_ref=self.target.at[self.base + self.me],
                 send_sem=self.send.at[k],
                 recv_sem=self.recv.at[k],
                 device_id={self.axis: peer},
             )
             copy.start()
             self.copies.append(copy)
-        self.target[self.me] = self.source(self.me)[...]
+        self.target[self.base + self.me] = self.source(self.me)[...]
 
     def arrive(self):
         for copy in self.copies:
@@ -508,37 +508,46 @@
         mixed_ref[places[b], :] = (centers[b] * lax.rsqrt(spreads[b] + GN_EPS) * gain).astype(bf16)
 
 
-def routing(routes_ref, weights_ref, room, capacity):
+def routing(routes_ref, weights_ref):
     rows = routes_ref.shape[1]
     slot = iota((rows, LANES), 1)
-    within = slot % room
-    second = (within >= capacity).astype(jnp.int32)
-    rank = within - second * capacity
-    in_use = within < 2 * capacity
-    expert = (slot // room * 2 + second).astype(f32)
-    named = []
+    names, values = [], []
     for k in range(2):
         pick = jnp.full((1, LANES), k, jnp.int32)
-        named.append(
-            (
-                jnp.where((to_columns(routes_ref[...].astype(f32), pick) == expert) & in_use, 1.0, 0.0),
-                to_columns(weights_ref[...], pick),
-            )
-        )
-    either = named[0][0] + named[1][0]
+        names.append(to_columns(routes_ref[...].astype(f32), pick))
+        values.append(to_columns(weights_ref[...], pick))
     before = (iota((rows, rows), 0) > iota((rows, rows), 1)).astype(bf16)
-    taken = raw_dot(before, either.astype(bf16), NN)
-    here = jnp.where(taken == rank.astype(f32), 1.0, 0.0)
-    placing = (either * here).astype(bf16)
-    weighting = (named[0][0] * named[0][1] + named[1][0] * named[1][1]) * here
-    per_expert = LANES // room * capacity
+
+    def filled(expert, rank):
+        named = [jnp.where(name == expert.astype(f32), 1.0, 0.0) for name in names]
+        either = named[0] + named[1]
+        taken = raw_dot(before, either.astype(bf16), NN)
+        here = jnp.where(taken == rank.astype(f32), 1.0, 0.0)
+        return either * here, (named[0] * values[0] + named[1] * values[1]) * here
+
+    placing, weighting = filled(slot // 8 * 2 + slot % 4 // 2, slot % 2)
+    late, late_weight = filled(slot % 32, jnp.full_like(slot, 2))
+    high, low = halves(late_weight)
+    kind = slot // 32
+    info = jnp.where(
+        kind == 0,
+        late,
+        jnp.where(kind == 1, high.astype(f32), jnp.where(kind == 2, low.astype(f32), 0.0)),
+    )
+    per_expert = LANES // 8 * 2
     shape = (2 * per_expert, LANES)
-    slot = iota(shape, 1)
-    within = slot % room
-    second = (within >= capacity).astype(jnp.int32)
-    target = second * per_expert + slot // room * capacity + within - second * capacity
-    packing = jnp.where((iota(shape, 0) == target) & (within < 2 * capacity), 1.0, 0.0).astype(bf16)
-    return placing, weighting, packing
+    at = iota(shape, 1)
+    target = at % 4 // 2 * per_expert + at // 8 * 2 + at % 2
+    column = at % 8 // 4
+    packing = [
+        jnp.where((iota(shape, 0) == target) & (column == k), 1.0, 0.0).astype(bf16) for k in range(2)
+    ]
+    return placing, weighting, info, packing
+
+
+def late_pick(lanes_per_part, part, core, peers, blocks):
+    row, lane = iota((peers * blocks, LANES), 0), iota((peers * blocks, LANES), 1)
+    return jnp.where(lane == part * lanes_per_part + row // blocks * 2 + core, 1.0, 0.0).astype(bf16)
 
 
 def layer_kernel(
@@ -579,6 +588,12 @@
     returned,
     shared_blocks,
     routed_blocks,
+    late_out,
+    late_blocks,
+    late_partial,
+    late_other,
+    late_back,
+    late_returned,
     mix_partial,
     shared_partial,
     routed_partial,
@@ -599,7 +614,6 @@
     ring = Ring(TP, devices // 2)
     local_experts = expert_gate.shape[0]
     width = input_ref.shape[1]
-    capacity, room = 3, outgoing.shape[1]
     used = packed.shape[0] // local_experts
     weight_copies = []
     for k, (pair, single, into) in enumerate(
@@ -617,7 +631,10 @@
         SP, sp_count, [(TP, ring.next[0]), (TP, ring.next[1]), (TP, ring.twin)]
     )
 
-    placing, weighting, packing = routing(routes_ref, route_weights_ref, room, capacity)
+    placing, weighting, info, packing = routing(routes_ref, route_weights_ref)
+    slot = iota(placing.shape, 1)
+    columns_of = [(slot % 8 // 4 == k).astype(f32) for k in range(2)]
+    side = width // 2
     mixer_stage(
         read_ref,
         key_ref,
@@ -638,6 +655,7 @@
     here = lax.axis_index(SP)
     states = Push(
         SP,
+        sp_count,
         lambda peer: whole_ref.at[(here + sp_count - peer) // (sp_count + 1)],
         got_ref,
         sems[24:26],
@@ -669,28 +687,34 @@
         rows = input_ref[piece, :].astype(f32) + mix_sum.own_half(which)
         residual[piece, :] = rows
         scale = lax.rsqrt(jnp.mean(rows * rows, axis=-1, keepdims=True) + RMS_EPS)
-        normed[piece, :] = (rows * scale * norm_gain).astype(bf16)
+        normed[piece, :width] = (rows * scale * norm_gain).astype(bf16)
+        normed[piece, width:] = info[piece, :].astype(bf16)
 
     shared_in = Gather(ring, normed, shared_blocks, sems[4:8])
     outgoing[...] = (
-        raw_dot(placing, normed[...], TN).astype(bf16).reshape(outgoing.shape)
+        raw_dot(
+            jnp.concatenate([(placing * c).astype(bf16) for c in columns_of], axis=0),
+            jnp.concatenate([normed[:, :side], normed[:, side:width]], axis=0),
+            TN,
+        )
+        .astype(bf16)
+        .reshape(outgoing.shape)
     )
     shared_in.begin()
-    dispatch = Push(SP, lambda peer: outgoing.at[peer], arrived, sems[8:10])
+    dispatch = Push(SP, sp_count, lambda peer: outgoing.at[peer], arrived, sems[8:10])
     dispatch.begin()
     for step in range(ring.steps - 1):
         shared_in.advance(step)
     dispatch.arrive()
-    packed[...] = raw_dot(
-        packing, arrived[...].reshape(packing.shape[1], width), NN
-    ).astype(bf16)
+    arrivals = arrived[...].reshape(LANES, side)
+    packed[...] = jnp.concatenate([raw_dot(p, arrivals, NN) for p in packing], axis=1).astype(bf16)
     routed_in = Gather(ring, packed, routed_blocks, sems[10:14])
     routed_in.begin()
     shared_in.advance(ring.steps - 1)
 
     def expert_on(blocks, partial, first, count, at, which):
         rows = at.size
-        x = blocks[pl.ds(first, count), at, :].reshape(count * rows, width)
+        x = blocks[pl.ds(first, count), at, pl.ds(0, width)].reshape(count * rows, width)
         gated = raw_dot(x, gate[which], NN)
         lifted = raw_dot(x, up[which], NN)
         inner = (gated / (1.0 + jnp.exp(-gated)) * lifted).astype(bf16)
@@ -715,10 +739,52 @@
 
     routed_sum = Sum(ring, routed_partial, routed_other, routed_inbox, sems[14:18])
     shared_sum = Sum(ring, shared_partial, shared_other, shared_inbox, sems[18:22])
+    shared_in.hand_own().wait_recv()
+    shared_in.handed(*range(ring.steps))
+
+    block_rows = normed.shape[0]
+    group_rows, late_rows = devices * block_rows, sp_count * devices
+    infos = shared_blocks[:, :, pl.ds(width, LANES)].reshape(group_rows, LANES)
+    of_block = (
+        iota((late_rows, group_rows), 0) % devices == iota((late_rows, group_rows), 1) // block_rows
+    )
+    chosen = jnp.where(
+        of_block, raw_dot(late_pick(32, 0, ring.core, sp_count, devices), infos, NT), 0.0
+    ).astype(bf16)
+
+    def choose(k, _):
+        at = pl.ds(pl.multiple_of(k * columns, columns), columns)
+        rows = raw_dot(chosen, shared_blocks[:, :, at].reshape(group_rows, columns), NN)
+        late_out[:, :, at] = rows.astype(bf16).reshape(sp_count, devices, columns)
+        return 0
+
+    lax.fori_loop(0, width // columns, choose, 0)
+    late_in = Push(
+        SP, sp_count, lambda peer: late_out.at[peer], late_blocks, sems[26:28], ring.core * sp_count
+    )
+    late_in.begin()
+
+    def late_hand(which):
+        return ring.copy(
+            late_blocks.at[which],
+            late_blocks.at[which],
+            sems[28].at[lax.rem(which, sp_count)],
+            sems[29].at[lax.rem(which, sp_count)],
+            ring.twin,
+        )
+
+    def late_handed(k):
+        return late_hand((1 - ring.core) * sp_count + k)
+
+    late_pair = ring.copy(
+        late_partial.at[pl.ds((1 - ring.core) * sp_count, sp_count)],
+        late_other,
+        sems[30].at[0],
+        sems[30].at[1],
+        ring.twin,
+    )
     for copy in weight_copies:
         copy.wait()
-    shared_in.hand_own().wait_recv()
-    shared_in.handed(*range(ring.steps))
 
     def quarters(first):
         def one(k, _):
@@ -749,33 +815,79 @@
             routed_sum.give(0, -2, 2)
         elif step == 6:
             routed_sum.give(-3, 3)
+    ring.start(late_hand(ring.core * sp_count + here))
+    for k in range(1, sp_count):
+        late_in.copies[k - 1].wait_recv()
+        ring.start(late_hand(ring.core * sp_count + lax.rem(here + sp_count - k, sp_count)))
     routed_in.handed(ring.steps - 1)
     routed_on(ring.far)
     routed_sum.give(ring.far)
+    routed_sum.advance(0)
+    routed_sum.advance(1)
+    for k in range(sp_count):
+        late_handed(k).wait_recv()
+
+    def late_on(k, _):
+        expert_on(late_blocks, late_partial, k * sp_count, sp_count, pl.ds(0, devices), k)
+        return 0
+
+    lax.fori_loop(0, local_experts, late_on, 0)
+    routed_sum.advance(2)
+    ring.start(late_pair)
+    routed_sum.advance(3)
+    late_pair.wait_recv()
+    late_back[...] = (
+        late_partial[pl.ds(ring.core * sp_count, sp_count)].astype(f32) + late_other[...].astype(f32)
+    ).astype(bf16)
+    late_home = Push(SP, sp_count, lambda peer: late_back.at[peer], late_returned, sems[31:33])
+    late_home.begin()
+    for step in range(4, ring.steps):
+        routed_sum.advance(step)
+    summed = jnp.concatenate([routed_sum.own_half(which).astype(bf16) for which in (0, 1)], axis=0)
+    unpacked[...] = (
+        (
+            raw_dot(packing[0], summed[:, :side], TN) + raw_dot(packing[1], summed[:, side:], TN)
+        )
+        .astype(bf16)
+        .reshape(unpacked.shape)
+    )
+    back = Push(SP, sp_count, lambda peer: unpacked.at[peer], returned, sems[22:24])
+    back.begin()
+    late_home.arrive()
+    by_row = iota((group_rows, late_rows), 0) // block_rows == iota((group_rows, late_rows), 1) % devices
+    late_weights = [
+        jnp.where(by_row, raw_dot(infos, late_pick(32, k, ring.core, sp_count, devices), NT), 0.0).astype(bf16)
+        for k in (1, 2)
+    ]
+
+    def add_late(k, _):
+        at = pl.ds(pl.multiple_of(k * columns, columns), columns)
+        rows = late_returned[:, :, at].reshape(late_rows, columns)
+        added = raw_dot(late_weights[0], rows, NN) + raw_dot(late_weights[1], rows, NN)
+        shared_partial[:, :, at] = (
+            shared_partial[:, :, at].astype(f32) + added.reshape(devices, block_rows, columns)
+        ).astype(bf16)
+        return 0
+
+    lax.fori_loop(0, width // columns, add_late, 0)
     shared_sum.give(ring.far, ring.far - 1, 1 - ring.far, *range(ring.far - 2, 1 - ring.far, -1))
     for step in range(ring.steps):
-        routed_sum.advance(step)
-    shared_sum.advance(0)
-    shared_sum.advance(1)
-    summed = jnp.concatenate([routed_sum.own_half(which).astype(bf16) for which in (0, 1)], axis=0)
-    unpacked[...] = raw_dot(packing, summed, TN).astype(bf16).reshape(unpacked.shape)
-    back = Push(SP, lambda peer: unpacked.at[peer], returned, sems[22:24])
-    back.begin()
-    for step in range(2, ring.steps):
         shared_sum.advance(step)
     half = residual.shape[0] // 2
     for which in (0, 1):
         piece = slice(which * half, (which + 1) * half)
         residual[piece, :] = residual[piece, :] + shared_sum.own_half(which)
     back.arrive()
-    rows = returned[...].reshape(weighting.shape[1], width)
-    routed = exact_right_dot(weighting, rows, NN)
+    rows = returned[...].reshape(LANES, side)
+    routed = jnp.concatenate([exact_right_dot(weighting * c, rows, NN) for c in columns_of], axis=1)
     o_ref[...] = (residual[...] + routed).astype(bf16)
     for copy in ring.sent:
         copy.wait_send()
     dispatch.leave()
     back.leave()
     states.leave()
+    late_in.leave()
+    late_home.leave()
 
 
 def layer(arrays, weights, devices, sp_count, capacity, room, number, name):
@@ -810,14 +922,20 @@
             buffer(sp_count, 2 * BLOCK, LANES),
             buffer(tokens, LANES),
             pltpu.VMEM((rows, width), f32),
-            buffer(rows, width),
-            buffer(sp_count, room, width),
-            buffer(sp_count, room, width),
+            buffer(rows, width + LANES),
+            buffer(sp_count, room, width // 2),
+            buffer(sp_count, room, width // 2),
             buffer(packed_rows, width),
-            buffer(sp_count, room, width),
-            buffer(sp_count, room, width),
-            buffer(devices, rows, width),
+            buffer(sp_count, room, width // 2),
+            buffer(sp_count, room, width // 2),
+            buffer(devices, rows, width + LANES),
             buffer(devices, packed_rows, width),
+            buffer(sp_count, devices, width),
+            buffer(local_experts * sp_count, devices, width),
+            buffer(local_experts * sp_count, devices, width),
+            buffer(sp_count, devices, width),
+            buffer(sp_count, devices, width),
+            buffer(sp_count, devices, width),
             buffer(devices, rows, width),
             buffer(devices, rows, width),
             buffer(devices, packed_rows, width),
@@ -839,6 +957,10 @@
         + sum_sems
         + sum_sems
         + push_sems
+        + push_sems
+        + push_sems
+        + push_sems
+        + [dma((2,))]
         + push_sems,
         compiler_params=pltpu.CompilerParams(
             collective_id=number, has_side_effects=True, vmem_limit_bytes=62 * 1024 * 1024
@@ -892,7 +1014,7 @@
         ),
         tp_count,
         sp_count,
-        3,
+        2,
         8,
         0,
         "layer",

time: 146 us -> 139 us (0.952)
  Pallas kernels: 144 us -> 137 us
    pallas_call x1, Pallas kernels: 144 us -> 137 us  [layer(): pl.pallas_call(functools.partial(layer_kernel, devices=devices, sp_count=...]
where the time goes in v5:
time: 139 us
  Pallas kernels  137 us (99%)
  local copies, waits for them, and re-layouts  1.57 us (1%)
    pallas_call x1, Pallas kernels, layer(): pl.pallas_call(functools.partial(layer_kernel, devices=devices, sp_count=...  137 us

profile of v5, /device:TPU:6, one launch (start us, length us, event | category | flops | bytes accessed | tf_op | source)
XLA Modules:
  0.0 138.8 jit_solution(8479136711168784140)
XLA Ops:
  0.0 137.2 %layer.1 = bf16[32,2048]{1,0:T(8,128)(2,1)} custom-call(bf16[512,128]{1,0:T(8,128)(2,1)} %read_ref.1, bf16[512,128]{1,0:T(8,128)(2,1)} %key_ref.1, bf16[512,128]{1,0:T(8,128)(2,1)} %value_ref.1, bf16[512,128]{1,0:T(8,128)(2,1)} %erase_ref.1, bf16[512,128]{1,0:T(8,128)(2,1)} %decay_ref.1, f32[2,512]{1,0:T(2,128)} %bitcast.5, bf16[1,128]{1,0:T(2,128)(2,1)} %bitcast.9, ...), custom_call_target="tpu_custom_call" | custom-call | tf_op jit(solution)/shard_map/layer/pallas_call | solution.py:908
  137.2 1.6 %copy.20 = bf16[32,2048]{1,0:T(8,128)(2,1)} copy(bf16[32,2048]{1,0:T(8,128)(2,1)} %layer.1) | data formatting | bytes 262144

commit v6 on v5

--- a/solution.py
+++ b/solution.py
@@ -374,9 +374,13 @@
         for distance in distances:
             self.ring.start(self.pair(distance))
 
+    def block(self, distance):
+        ring = self.ring
+        return ring.chip_at(distance) if self.other is None else ring.slot(distance, ring.core)
+
     def meet(self, distance):
         key = distance % self.ring.chips
-        if key not in self.met:
+        if self.other is not None and key not in self.met:
             self.met.add(key)
             self.pair(distance).wait_recv()
 
@@ -389,7 +393,7 @@
         ring = self.ring
         distance, piece = self.place(way, step)
         return ring.copy(
-            self.partial.at[ring.slot(distance, ring.core), piece],
+            self.partial.at[self.block(distance), piece],
             self.inbox.at[way, step],
             self.send_sem.at[way, step],
             self.recv_sem.at[way, step],
@@ -397,10 +401,10 @@
         )
 
     def both_cores(self, distance, piece):
-        ring = self.ring
-        return self.partial[ring.slot(distance, ring.core), piece, :].astype(f32) + self.other[
-            ring.chip_at(distance), piece, :
-        ].astype(f32)
+        rows = self.partial[self.block(distance), piece, :].astype(f32)
+        if self.other is None:
+            return rows
+        return rows + self.other[self.ring.chip_at(distance), piece, :].astype(f32)
 
     def advance(self, step):
         ring = self.ring
@@ -411,7 +415,7 @@
             if step >= 2:
                 self.hop(way, step - 2).wait_recv()
                 total = total + self.inbox[way, step - 2].astype(f32)
-            self.partial[ring.slot(distance, ring.core), piece, :] = total.astype(bf16)
+            self.partial[self.block(distance), piece, :] = total.astype(bf16)
         for way in (0, 1):
             ring.start(self.hop(way, step))
 
@@ -462,21 +466,27 @@
     barrier = pltpu.get_barrier_semaphore()
     for k in range(1, count):
         pl.semaphore_signal(barrier, inc=1, device_id={axis: lax.rem(me + k, count)})
-    for name, peer in others:
-        pl.semaphore_signal(barrier, inc=1, device_id={name: peer})
+    for peer in others:
+        pl.semaphore_signal(barrier, inc=1, device_id=peer)
     return barrier, count - 1 + len(others)
 
 
-def finish_blocks(place, got_ref, local_ref, readout_ref, prefix_ref, start_ref, gain_ref, mixed_ref):
-    count = got_ref.shape[0]
+def finish_blocks(
+    place, await_state, got_ref, local_ref, readout_ref, prefix_ref, start_ref, gain_ref, mixed_ref
+):
+    last = got_ref.shape[0] - 1
     blocks = range(prefix_ref.shape[1])
-    entry = [jnp.zeros((BLOCK, LANES), f32)] * 2
-    for k in range(count - 1):
-        for way in range(2):
-            j = k if way == 0 else count - 1 - k
-            passed = j < place if way == 0 else j > place
-            moved = exact_right_dot(entry[way], both_heads(got_ref[j, :BLOCK, :]), NN)
-            entry[way] = jnp.where(passed, moved + got_ref[j, BLOCK:, :].astype(f32), entry[way])
+
+    def after(j, entry):
+        await_state(j)
+        moved = exact_right_dot(entry, both_heads(got_ref[j, :BLOCK, :]), NN)
+        return moved + got_ref[j, BLOCK:, :].astype(f32)
+
+    blank = jnp.zeros((BLOCK, LANES), f32)
+    entry = [
+        lax.fori_loop(0, place, after, blank),
+        lax.fori_loop(0, last - place, lambda k, e: after(last - k, e), blank),
+    ]
     gain = gain_ref[...].astype(f32)
     states = []
     for way in range(2):
@@ -505,7 +515,8 @@
     centers = [mix - head_sum(mix) * (1.0 / BLOCK) for mix in mixes]
     spreads = [head_sum(center * center) * (1.0 / BLOCK) for center in centers]
     for b in blocks:
-        mixed_ref[places[b], :] = (centers[b] * lax.rsqrt(spreads[b] + GN_EPS) * gain).astype(bf16)
+        rows = (centers[b] * lax.rsqrt(spreads[b] + GN_EPS) * gain).astype(bf16)
+        mixed_ref[b] = rows.reshape(mixed_ref.shape[1:])
 
 
 def routing(routes_ref, weights_ref):
@@ -545,9 +556,9 @@
     return placing, weighting, info, packing
 
 
-def late_pick(lanes_per_part, part, core, peers, blocks):
+def late_pick(core, peers, blocks):
     row, lane = iota((peers * blocks, LANES), 0), iota((peers * blocks, LANES), 1)
-    return jnp.where(lane == part * lanes_per_part + row // blocks * 2 + core, 1.0, 0.0).astype(bf16)
+    return jnp.where(lane == row // blocks * 2 + core, 1.0, 0.0).astype(bf16)
 
 
 def layer_kernel(
@@ -594,10 +605,12 @@
     late_other,
     late_back,
     late_returned,
+    mix_weight_other,
+    mixed_other,
+    shared_chip,
     mix_partial,
     shared_partial,
     routed_partial,
-    mix_other,
     shared_other,
     routed_other,
     mix_inbox,
@@ -628,7 +641,12 @@
     for copy in weight_copies:
         copy.start()
     barrier, expected = meet_peers(
-        SP, sp_count, [(TP, ring.next[0]), (TP, ring.next[1]), (TP, ring.twin)]
+        SP,
+        sp_count,
+        [{TP: ring.next[0]}, {TP: ring.next[1]}, {TP: ring.twin}]
+        + [
+            {SP: lax.rem(lax.axis_index(SP) + k, sp_count), TP: ring.twin} for k in range(1, sp_count)
+        ],
     )
 
     placing, weighting, info, packing = routing(routes_ref, route_weights_ref)
@@ -661,22 +679,44 @@
         sems[24:26],
     )
     states.begin()
-    states.arrive()
+    twin_weight = ring.copy(
+        mix_weight_ref, mix_weight_other, sems[33].at[0], sems[33].at[1], ring.twin
+    )
+    ring.start(twin_weight)
+
+    def await_state(j):
+        k = lax.rem(here + sp_count - j, sp_count)
+        pltpu.make_async_remote_copy(
+            src_ref=whole_ref.at[0],
+            dst_ref=got_ref.at[j],
+            send_sem=sems[24].at[k],
+            recv_sem=sems[25].at[k],
+            device_id={SP: j},
+        ).wait_recv()
 
     finish_blocks(
-        lax.axis_index(SP), got_ref, local_ref, readout_ref, prefix_ref, start_ref, gain_ref, mixed
-    )
+        here, await_state, got_ref, local_ref, readout_ref, prefix_ref, start_ref, gain_ref, mixed
+    )
+    twin_mixed = ring.copy(
+        mixed.at[:, 1 - ring.core], mixed_other, sems[33].at[2], sems[33].at[3], ring.twin
+    )
+    ring.start(twin_mixed)
     columns = 512
+    own_rows = mix_partial.shape[0] * mix_partial.shape[1]
+    twin_weight.wait_recv()
+    own_mixed = mixed[:, ring.core].reshape(own_rows, LANES)
+    twin_mixed.wait_recv()
+    heads = jnp.concatenate([own_mixed, mixed_other[...].reshape(own_rows, LANES)], axis=1)
 
     def project(k, _):
         at = pl.ds(pl.multiple_of(k * columns, columns), columns)
-        product = raw_dot(mixed[...], mix_weight_ref[:, at], NN).astype(bf16)
+        weight = jnp.concatenate([mix_weight_ref[:, at], mix_weight_other[:, at]], axis=0)
+        product = raw_dot(heads, weight, NN).astype(bf16)
         mix_partial[:, :, at] = product.reshape(mix_partial.shape[0], mix_partial.shape[1], columns)
         return 0
 
     lax.fori_loop(0, width // columns, project, 0)
-    mix_sum = Sum(ring, mix_partial, mix_other, mix_inbox, sems[0:4])
-    mix_sum.give(ring.far, ring.far - 1, 1 - ring.far, *range(ring.far - 2, 1 - ring.far, -1))
+    mix_sum = Sum(ring, mix_partial, None, mix_inbox, sems[0:4])
     for step in range(ring.steps):
         mix_sum.advance(step)
     gains = norm_gain_ref[...].astype(f32)
@@ -703,53 +743,64 @@
     shared_in.begin()
     dispatch = Push(SP, sp_count, lambda peer: outgoing.at[peer], arrived, sems[8:10])
     dispatch.begin()
-    for step in range(ring.steps - 1):
+    for step in range(ring.steps - 2):
         shared_in.advance(step)
     dispatch.arrive()
     arrivals = arrived[...].reshape(LANES, side)
     packed[...] = jnp.concatenate([raw_dot(p, arrivals, NN) for p in packing], axis=1).astype(bf16)
     routed_in = Gather(ring, packed, routed_blocks, sems[10:14])
     routed_in.begin()
+    shared_in.advance(ring.steps - 2)
     shared_in.advance(ring.steps - 1)
 
-    def expert_on(blocks, partial, first, count, at, which):
+    def expert_on(blocks, partial, firsts, count, at, which):
         rows = at.size
-        x = blocks[pl.ds(first, count), at, pl.ds(0, width)].reshape(count * rows, width)
+        x = jnp.concatenate(
+            [
+                blocks[pl.ds(first, count), at, pl.ds(0, width)].reshape(count * rows, width)
+                for first in firsts
+            ],
+            axis=0,
+        )
         gated = raw_dot(x, gate[which], NN)
         lifted = raw_dot(x, up[which], NN)
         inner = (gated / (1.0 + jnp.exp(-gated)) * lifted).astype(bf16)
-        partial[pl.ds(first, count), at, :] = (
-            raw_dot(inner, down[which], NN).astype(bf16).reshape(count, rows, width)
-        )
-
-    def routed_on(distance):
-        first = ring.chip_at(distance) * 2
+        outer = raw_dot(inner, down[which], NN).astype(bf16)
+        for k, first in enumerate(firsts):
+            partial[pl.ds(first, count), at, :] = outer[
+                k * count * rows : (k + 1) * count * rows
+            ].reshape(count, rows, width)
+
+    def routed_on(*distances):
+        firsts = [ring.chip_at(distance) * 2 for distance in distances]
 
         def one(k, _):
             at = pl.ds(pl.multiple_of(k * used, 16), used)
-            expert_on(routed_blocks, routed_partial, first, 2, at, k)
+            expert_on(routed_blocks, routed_partial, firsts, 2, at, k)
             return 0
 
         lax.fori_loop(0, local_experts, one, 0)
 
-    def shared_on(quarter):
-        count = devices // 4
+    def shared_half(which):
+        count = devices // 2
         at = pl.ds(0, normed.shape[0])
-        expert_on(shared_blocks, shared_partial, quarter * count, count, at, local_experts)
+        expert_on(shared_blocks, shared_partial, [which * count], count, at, local_experts)
 
     routed_sum = Sum(ring, routed_partial, routed_other, routed_inbox, sems[14:18])
-    shared_sum = Sum(ring, shared_partial, shared_other, shared_inbox, sems[18:22])
+    shared_pairs = Sum(ring, shared_partial, shared_other, None, sems[18:20] + (None, None))
+    shared_sum = Sum(ring, shared_chip, None, shared_inbox, (None, None) + sems[20:22])
     shared_in.hand_own().wait_recv()
     shared_in.handed(*range(ring.steps))
 
     block_rows = normed.shape[0]
     group_rows, late_rows = devices * block_rows, sp_count * devices
     infos = shared_blocks[:, :, pl.ds(width, LANES)].reshape(group_rows, LANES)
+    order = iota((late_rows, group_rows), 0) % devices
     of_block = (
-        iota((late_rows, group_rows), 0) % devices == iota((late_rows, group_rows), 1) // block_rows
+        order % ring.chips * 2 + order // ring.chips == iota((late_rows, group_rows), 1) // block_rows
     )
     chosen = jnp.where(
-        of_block, raw_dot(late_pick(32, 0, ring.core, sp_count, devices), infos, NT), 0.0
+        of_block, raw_dot(late_pick(ring.core, sp_count, devices), infos, NT), 0.0
     ).astype(bf16)
 
     def choose(k, _):
@@ -786,35 +837,24 @@
     for copy in weight_copies:
         copy.wait()
 
-    def quarters(first):
-        def one(k, _):
-            shared_on(first + k)
-            return 0
-
-        lax.fori_loop(0, 2, one, 0)
-
-    quarters(0)
+    shared_half(0)
     for step in range(ring.steps):
         routed_in.advance(step)
         if step == 0:
-            quarters(2)
+            shared_half(1)
+        elif step == 1:
+            shared_pairs.give(*range(ring.chips))
+            routed_in.hand_own().wait_recv()
+            routed_in.handed(0, 1)
+            routed_on(0, -1, 1)
+        elif step == 2:
+            routed_sum.give(0, -1, 1)
         elif step % 2 == 1:
             distance = (step + 1) // 2
             routed_in.handed(step - 1, step)
-
-            def both(k, _):
-                routed_on(distance * (2 * k - 1))
-                return 0
-
-            lax.fori_loop(0, 2, both, 0)
-        elif step == 2:
-            routed_in.hand_own().wait_recv()
-            routed_on(0)
-            routed_sum.give(-1, 1)
-        elif step == 4:
-            routed_sum.give(0, -2, 2)
-        elif step == 6:
-            routed_sum.give(-3, 3)
+            routed_on(-distance, distance)
+        else:
+            routed_sum.give(-(step // 2), step // 2)
     ring.start(late_hand(ring.core * sp_count + here))
     for k in range(1, sp_count):
         late_in.copies[k - 1].wait_recv()
@@ -828,7 +868,7 @@
         late_handed(k).wait_recv()
 
     def late_on(k, _):
-        expert_on(late_blocks, late_partial, k * sp_count, sp_count, pl.ds(0, devices), k)
+        expert_on(late_blocks, late_partial, [k * sp_count], sp_count, pl.ds(0, devices), k)
         return 0
 
     lax.fori_loop(0, local_experts, late_on, 0)
@@ -837,10 +877,31 @@
     routed_sum.advance(3)
     late_pair.wait_recv()
     late_back[...] = (
-        late_partial[pl.ds(ring.core * sp_count, sp_count)].astype(f32) + late_other[...].astype(f32)
-    ).astype(bf16)
-    late_home = Push(SP, sp_count, lambda peer: late_back.at[peer], late_returned, sems[31:33])
-    late_home.begin()
+        (
+            late_partial[pl.ds(ring.core * sp_count, sp_count)].astype(f32)
+            + late_other[...].astype(f32)
+        )
+        .reshape(late_back.shape)
+        .astype(bf16)
+    )
+    at_home = ring.core * sp_count + here
+    late_home = []
+    for k in range(sp_count):
+        for same in (0, 1):
+            core = ring.core if same == 0 else 1 - ring.core
+            peer = lax.rem(here + k, sp_count)
+            if k == 0 and same == 0:
+                late_returned[at_home] = late_back[here, core]
+                continue
+            copy = pltpu.make_async_remote_copy(
+                src_ref=late_back.at[peer, core],
+                dst_ref=late_returned.at[at_home],
+                send_sem=sems[31].at[same, k],
+                recv_sem=sems[32].at[same, k],
+                device_id={SP: peer, TP: ring.chip * 2 + core},
+            )
+            ring.start(copy)
+            late_home.append(copy)
     for step in range(4, ring.steps):
         routed_sum.advance(step)
     summed = jnp.concatenate([routed_sum.own_half(which).astype(bf16) for which in (0, 1)], axis=0)
@@ -853,24 +914,39 @@
     )
     back = Push(SP, sp_count, lambda peer: unpacked.at[peer], returned, sems[22:24])
     back.begin()
-    late_home.arrive()
-    by_row = iota((group_rows, late_rows), 0) // block_rows == iota((group_rows, late_rows), 1) % devices
+    own_slots = [2 * k + ring.core for k in range(ring.chips)]
+    own_infos = jnp.concatenate([shared_blocks[k, :, pl.ds(width, LANES)] for k in own_slots], axis=0)
+    column, lane = iota((late_rows, LANES), 0), iota((late_rows, LANES), 1)
+    wanted = column % LANES // ring.chips * 2 + column // LANES
+    shape = (own_rows, late_rows)
+    by_row = iota(shape, 0) // block_rows == iota(shape, 1) % ring.chips
     late_weights = [
-        jnp.where(by_row, raw_dot(infos, late_pick(32, k, ring.core, sp_count, devices), NT), 0.0).astype(bf16)
+        jnp.where(
+            by_row,
+            raw_dot(own_infos, jnp.where(lane == 32 * k + wanted, 1.0, 0.0).astype(bf16), NT),
+            0.0,
+        ).astype(bf16)
         for k in (1, 2)
     ]
+    for k in range(ring.chips):
+        shared_pairs.meet(k)
+    for copy in late_home:
+        copy.wait_recv()
 
     def add_late(k, _):
         at = pl.ds(pl.multiple_of(k * columns, columns), columns)
         rows = late_returned[:, :, at].reshape(late_rows, columns)
-        added = raw_dot(late_weights[0], rows, NN) + raw_dot(late_weights[1], rows, NN)
-        shared_partial[:, :, at] = (
-            shared_partial[:, :, at].astype(f32) + added.reshape(devices, block_rows, columns)
-        ).astype(bf16)
+        own = jnp.concatenate([shared_partial[slot, :, at] for slot in own_slots], axis=0).astype(f32)
+        total = (
+            own
+            + shared_other[:, :, at].reshape(own_rows, columns).astype(f32)
+            + raw_dot(late_weights[0], rows, NN)
+            + raw_dot(late_weights[1], rows, NN)
+        )
+        shared_chip[:, :, at] = total.astype(bf16).reshape(ring.chips, block_rows, columns)
         return 0
 
     lax.fori_loop(0, width // columns, add_late, 0)
-    shared_sum.give(ring.far, ring.far - 1, 1 - ring.far, *range(ring.far - 2, 1 - ring.far, -1))
     for step in range(ring.steps):
         shared_sum.advance(step)
     half = residual.shape[0] // 2
@@ -887,7 +963,6 @@
     back.leave()
     states.leave()
     late_in.leave()
-    late_home.leave()
 
 
 def layer(arrays, weights, devices, sp_count, capacity, room, number, name):
@@ -920,7 +995,7 @@
             pltpu.VMEM((2, block_count, BLOCK, LANES), f32),
             buffer(2, 2 * BLOCK, LANES),
             buffer(sp_count, 2 * BLOCK, LANES),
-            buffer(tokens, LANES),
+            buffer(chips, 2, rows, LANES),
             pltpu.VMEM((rows, width), f32),
             buffer(rows, width + LANES),
             buffer(sp_count, room, width // 2),
@@ -934,12 +1009,14 @@
             buffer(local_experts * sp_count, devices, width),
             buffer(local_experts * sp_count, devices, width),
             buffer(sp_count, devices, width),
-            buffer(sp_count, devices, width),
-            buffer(sp_count, devices, width),
-            buffer(devices, rows, width),
+            buffer(sp_count, 2, chips, width),
+            buffer(2 * sp_count, chips, width),
+            buffer(LANES, width),
+            buffer(chips, rows, LANES),
+            buffer(chips, rows, width),
+            buffer(chips, rows, width),
             buffer(devices, rows, width),
             buffer(devices, packed_rows, width),
-            buffer(chips, rows, width),
             buffer(chips, rows, width),
             buffer(chips, packed_rows, width),
             buffer(2, steps, rows // 2, width),
@@ -960,8 +1037,7 @@
         + push_sems
         + push_sems
         + push_sems
-        + [dma((2,))]
-        + push_sems,
+        + [dma((2,)), dma((2, sp_count)), dma((2, sp_count)), dma((4,))],
         compiler_params=pltpu.CompilerParams(
             collective_id=number, has_side_effects=True, vmem_limit_bytes=62 * 1024 * 1024
         ),

time: 139 us -> 135 us (0.971)
  Pallas kernels: 137 us -> 134 us
    pallas_call x1, Pallas kernels: 137 us -> 134 us  [layer(): pl.pallas_call(functools.partial(layer_kernel, devices=devices, sp_count=...]
where the time goes in v6:
time: 135 us
  Pallas kernels  134 us (99%)
  local copies, waits for them, and re-layouts  1.57 us (1%)
    pallas_call x1, Pallas kernels, layer(): pl.pallas_call(functools.partial(layer_kernel, devices=devices, sp_count=...  134 us

profile of v6, /device:TPU:6, one launch (start us, length us, event | category | flops | bytes accessed | tf_op | source)
XLA Modules:
  0.0 135.3 jit_solution(5848261801213080365)
XLA Ops:
  0.0 133.7 %layer.1 = bf16[32,2048]{1,0:T(8,128)(2,1)} custom-call(bf16[512,128]{1,0:T(8,128)(2,1)} %read_ref.1, bf16[512,128]{1,0:T(8,128)(2,1)} %key_ref.1, bf16[512,128]{1,0:T(8,128)(2,1)} %value_ref.1, bf16[512,128]{1,0:T(8,128)(2,1)} %erase_ref.1, bf16[512,128]{1,0:T(8,128)(2,1)} %decay_ref.1, f32[2,512]{1,0:T(2,128)} %bitcast.5, bf16[1,128]{1,0:T(2,128)(2,1)} %bitcast.9, ...), custom_call_target="tpu_custom_call" | custom-call | tf_op jit(solution)/shard_map/layer/pallas_call | solution.py:983
  133.7 1.6 %copy.20 = bf16[32,2048]{1,0:T(8,128)(2,1)} copy(bf16[32,2048]{1,0:T(8,128)(2,1)} %layer.1) | data formatting | bytes 262144

commit v7 on v6

--- a/solution.py
+++ b/solution.py
@@ -290,35 +290,44 @@
         return step % 2 if way == 0 else 1 - step % 2
 
 
+PARTS = 2
+
+
+def column_parts(width):
+    side = width // LANES // PARTS * LANES
+    return [pl.ds(0, side), pl.ds(side, width - side)]
+
+
 class Gather:
     def __init__(self, ring, own, blocks, sems):
         self.ring, self.own, self.blocks = ring, own, blocks
         self.send, self.recv, self.pass_send, self.pass_recv = sems
         self.half = own.shape[0] // 2
+        self.columns = column_parts(own.shape[1])
 
     def piece(self, way, step):
         return pl.ds(self.ring.half_of(way, step) * self.half, self.half)
 
-    def hop(self, way, step):
-        ring, piece = self.ring, self.piece(way, step)
+    def hop(self, way, step, part):
+        ring, piece, columns = self.ring, self.piece(way, step), self.columns[part]
         at = ring.slot((step // 2) * (-1 if way == 0 else 1), ring.core)
-        source = self.own.at[piece] if step < 2 else self.blocks.at[at, piece]
+        source = self.own.at[piece, columns] if step < 2 else self.blocks.at[at, piece, columns]
         return ring.copy(
             source,
-            self.blocks.at[at, piece],
-            self.send.at[way, step],
-            self.recv.at[way, step],
+            self.blocks.at[at, piece, columns],
+            self.send.at[way, step * PARTS + part],
+            self.recv.at[way, step * PARTS + part],
             ring.next[way],
         )
 
-    def hand(self, way, step):
-        ring, piece = self.ring, self.piece(way, step)
+    def hand(self, way, step, part):
+        ring, piece, columns = self.ring, self.piece(way, step), self.columns[part]
         at = ring.slot((step // 2 + 1) * (-1 if way == 0 else 1), ring.core)
         return ring.copy(
-            self.blocks.at[at, piece],
-            self.blocks.at[at, piece],
-            self.pass_send.at[way, step],
-            self.pass_recv.at[way, step],
+            self.blocks.at[at, piece, columns],
+            self.blocks.at[at, piece, columns],
+            self.pass_send.at[way, step * PARTS + part],
+            self.pass_recv.at[way, step * PARTS + part],
             ring.twin,
         )
 
@@ -327,29 +336,32 @@
         return ring.copy(
             self.own,
             self.blocks.at[ring.me],
-            self.pass_send.at[0, ring.steps],
-            self.pass_recv.at[0, ring.steps],
+            self.pass_send.at[0, ring.steps * PARTS],
+            self.pass_recv.at[0, ring.steps * PARTS],
             ring.twin,
         )
 
     def begin(self):
         for step in (0, 1):
-            for way in (0, 1):
-                self.ring.start(self.hop(way, step))
+            for part in range(PARTS):
+                for way in (0, 1):
+                    self.ring.start(self.hop(way, step, part))
         self.ring.start(self.hand_own())
         self.blocks[self.ring.me] = self.own[...]
 
     def advance(self, step):
-        for way in (0, 1):
-            self.hop(way, step).wait_recv()
-            if step + 2 < self.ring.steps:
-                self.ring.start(self.hop(way, step + 2))
-            self.ring.start(self.hand(way, step))
+        for part in range(PARTS):
+            for way in (0, 1):
+                self.hop(way, step, part).wait_recv()
+                if step + 2 < self.ring.steps:
+                    self.ring.start(self.hop(way, step + 2, part))
+                self.ring.start(self.hand(way, step, part))
 
     def handed(self, *steps):
         for step in steps:
-            for way in (0, 1):
-                self.hand(way, step).wait_recv()
+            for part in range(PARTS):
+                for way in (0, 1):
+                    self.hand(way, step, part).wait_recv()
 
 
 class Sum:
@@ -357,6 +369,7 @@
         self.ring, self.partial, self.other, self.inbox = ring, partial, other, inbox
         self.pair_send, self.pair_recv, self.send_sem, self.recv_sem = sems
         self.half = partial.shape[1] // 2
+        self.columns = column_parts(partial.shape[2])
         self.met = set()
 
     def pair(self, distance):
@@ -389,45 +402,52 @@
         distance = (ring.far - (step + 1) // 2) * (1 if way == 0 else -1)
         return distance, pl.ds(ring.half_of(way, step) * self.half, self.half)
 
-    def hop(self, way, step):
+    def hop(self, way, step, part):
         ring = self.ring
         distance, piece = self.place(way, step)
+        columns = self.columns[part]
         return ring.copy(
-            self.partial.at[self.block(distance), piece],
-            self.inbox.at[way, step],
-            self.send_sem.at[way, step],
-            self.recv_sem.at[way, step],
+            self.partial.at[self.block(distance), piece, columns],
+            self.inbox.at[way, step, :, columns],
+            self.send_sem.at[way, step * PARTS + part],
+            self.recv_sem.at[way, step * PARTS + part],
             ring.next[way],
         )
 
-    def both_cores(self, distance, piece):
-        rows = self.partial[self.block(distance), piece, :].astype(f32)
+    def both_cores(self, distance, piece, columns):
+        rows = self.partial[self.block(distance), piece, columns].astype(f32)
         if self.other is None:
             return rows
-        return rows + self.other[self.ring.chip_at(distance), piece, :].astype(f32)
+        return rows + self.other[self.ring.chip_at(distance), piece, columns].astype(f32)
 
     def advance(self, step):
         ring = self.ring
-        for way in (0, 1):
-            distance, piece = self.place(way, step)
-            self.meet(distance)
-            total = self.both_cores(distance, piece)
-            if step >= 2:
-                self.hop(way, step - 2).wait_recv()
-                total = total + self.inbox[way, step - 2].astype(f32)
-            self.partial[self.block(distance), piece, :] = total.astype(bf16)
-        for way in (0, 1):
-            ring.start(self.hop(way, step))
+        for part, columns in enumerate(self.columns):
+            for way in (0, 1):
+                distance, piece = self.place(way, step)
+                self.meet(distance)
+                if step >= 2 or self.other is not None:
+                    total = self.both_cores(distance, piece, columns)
+                    if step >= 2:
+                        self.hop(way, step - 2, part).wait_recv()
+                        total = total + self.inbox[way, step - 2, :, columns].astype(f32)
+                    self.partial[self.block(distance), piece, columns] = total.astype(bf16)
+            for way in (0, 1):
+                ring.start(self.hop(way, step, part))
 
     def own_half(self, which):
         ring = self.ring
         self.meet(0)
-        total = self.both_cores(0, pl.ds(which * self.half, self.half))
-        for way in (0, 1):
-            step = ring.steps - 2 if ring.half_of(way, ring.steps - 2) == which else ring.steps - 1
-            self.hop(way, step).wait_recv()
-            total = total + self.inbox[way, step].astype(f32)
-        return total
+        totals = []
+        for part, columns in enumerate(self.columns):
+            total = self.both_cores(0, pl.ds(which * self.half, self.half), columns)
+            for way in (0, 1):
+                even = ring.half_of(way, ring.steps - 2) == which
+                step = ring.steps - 2 if even else ring.steps - 1
+                self.hop(way, step, part).wait_recv()
+                total = total + self.inbox[way, step, :, columns].astype(f32)
+            totals.append(total)
+        return jnp.concatenate(totals, axis=1)
 
 
 class Push:
@@ -977,8 +997,9 @@
     dma = pltpu.SemaphoreType.DMA
     anywhere = pl.BlockSpec(memory_space=pl.ANY)
     buffer = lambda *shape: pltpu.VMEM(shape, bf16)
-    gather_sems = [dma((2, steps)), dma((2, steps)), dma((2, steps + 1)), dma((2, steps + 1))]
-    sum_sems = [dma((chips,)), dma((chips,)), dma((2, steps)), dma((2, steps))]
+    hops = steps * PARTS
+    gather_sems = [dma((2, hops)), dma((2, hops)), dma((2, hops + 1)), dma((2, hops + 1))]
+    sum_sems = [dma((chips,)), dma((chips,)), dma((2, hops)), dma((2, hops))]
     push_sems = [dma((sp_count,)), dma((sp_count,))]
     return pl.pallas_call(
         functools.partial(layer_kernel, devices=devices, sp_count=sp_count),

time: 135 us -> 132 us (0.978)
  Pallas kernels: 134 us -> 130 us
    pallas_call x1, Pallas kernels: 134 us -> 130 us  [layer(): pl.pallas_call(functools.partial(layer_kernel, devices=devices, sp_count=...]
where the time goes in v7:
time: 132 us; the launch traced here: 131 us
  Pallas kernels  130 us (98%)
  local copies, waits for them, and re-layouts  1.57 us (1%)
    pallas_call x1, Pallas kernels, layer(): pl.pallas_call(functools.partial(layer_kernel, devices=devices, sp_count=...  130 us

profile of v7, /device:TPU:6, one launch (start us, length us, event | category | flops | bytes accessed | tf_op | source)
XLA Modules:
  0.0 131.2 jit_solution(6894350141538612871)
XLA Ops:
  0.0 129.6 %layer.1 = bf16[32,2048]{1,0:T(8,128)(2,1)} custom-call(bf16[512,128]{1,0:T(8,128)(2,1)} %read_ref.1, bf16[512,128]{1,0:T(8,128)(2,1)} %key_ref.1, bf16[512,128]{1,0:T(8,128)(2,1)} %value_ref.1, bf16[512,128]{1,0:T(8,128)(2,1)} %erase_ref.1, bf16[512,128]{1,0:T(8,128)(2,1)} %decay_ref.1, f32[2,512]{1,0:T(2,128)} %bitcast.5, bf16[1,128]{1,0:T(2,128)(2,1)} %bitcast.9, ...), custom_call_target="tpu_custom_call" | custom-call | tf_op jit(solution)/shard_map/layer/pallas_call | solution.py:1004
  129.6 1.6 %copy.20 = bf16[32,2048]{1,0:T(8,128)(2,1)} copy(bf16[32,2048]{1,0:T(8,128)(2,1)} %layer.1) | data formatting | bytes 262144

commit v8 on v7

--- a/solution.py
+++ b/solution.py
@@ -687,7 +687,7 @@
         move_ref,
         carry_ref,
         whole_ref,
-        4,
+        8,
     )
     pl.semaphore_wait(barrier, expected)
     here = lax.axis_index(SP)

time: 132 us -> 130 us (0.985)
  Pallas kernels: 130 us -> 128 us
    pallas_call x1, Pallas kernels: 130 us -> 128 us  [layer(): pl.pallas_call(functools.partial(layer_kernel, devices=devices, sp_count=...]
where the time goes in v8:
time: 130 us
  Pallas kernels  128 us (98%)
  local copies, waits for them, and re-layouts  1.57 us (1%)
    pallas_call x1, Pallas kernels, layer(): pl.pallas_call(functools.partial(layer_kernel, devices=devices, sp_count=...  128 us

profile of v8, /device:TPU:6, one launch (start us, length us, event | category | flops | bytes accessed | tf_op | source)
XLA Modules:
  0.0 129.8 jit_solution(7547135887571605133)
XLA Ops:
  0.0 128.2 %layer.1 = bf16[32,2048]{1,0:T(8,128)(2,1)} custom-call(bf16[512,128]{1,0:T(8,128)(2,1)} %read_ref.1, bf16[512,128]{1,0:T(8,128)(2,1)} %key_ref.1, bf16[512,128]{1,0:T(8,128)(2,1)} %value_ref.1, bf16[512,128]{1,0:T(8,128)(2,1)} %erase_ref.1, bf16[512,128]{1,0:T(8,128)(2,1)} %decay_ref.1, f32[2,512]{1,0:T(2,128)} %bitcast.5, bf16[1,128]{1,0:T(2,128)(2,1)} %bitcast.9, ...), custom_call_target="tpu_custom_call" | custom-call | tf_op jit(solution)/shard_map/layer/pallas_call | solution.py:1004
  128.2 1.6 %copy.20 = bf16[32,2048]{1,0:T(8,128)(2,1)} copy(bf16[32,2048]{1,0:T(8,128)(2,1)} %layer.1) | data formatting | bytes 262144
